TPU v7x, 128 devices: a whole 4x4x4 slice. The times are simulated.
128 devices in a mesh: fs: 16 (over z, y), tp: 8 (over x, core).
Axes of the slice: x: 4, y: 4, z: 4, core: 2. Of those that a mesh axis runs over, the one named last changes fastest.
Arguments:
- tokens: bfloat16 [16384, 2048], P(('fs', 'tp')), may hold values from -6 to 6
- norm_gain: float32 [2048], replicated, may hold values from 0.1 to 1.9
- up_weight: float32 [2048, 8192], P('fs', 'tp'), may hold values from -0.125 to 0.125
- down_weight: float32 [8192, 2048], P('tp', 'fs'), may hold values from -0.0625 to 0.0625
Outputs:
- mlp_out: bfloat16 [16384, 2048], P(('fs', 'tp'))
All inputs are finite; a program needn't handle non-finite values.
Results may differ from a plain program's by a relative error of at most 0.0017.
Values may be sent and summed in bfloat16 or wider, within the bound.
A program may use at most 64 MiB of HBM per device.

v0:
```python
import jax
import jax.numpy as jnp
from jax import lax
from jax.sharding import PartitionSpec as P

epsilon = 1e-06


def taken_in(slab, axis, dim, step, start):
    def gathered(part):
        return lax.all_gather(part, axis, axis=dim, tiled=True)

    return step(start, jax.tree.map(gathered, slab), jnp.int32(0))


def on_whole(shard, axis, dim, work):
    return work(lax.all_gather(shard, axis, axis=dim, tiled=True), jnp.int32(0))


def shards(tokens, norm_gain, up_weight, down_weight):
    values = tokens.astype(jnp.float32)
    scale = lax.rsqrt(jnp.mean(values * values, axis=-1, keepdims=True) + epsilon)
    normed = (values * scale * norm_gain).astype(jnp.bfloat16)
    grouped = lax.all_gather(normed, "tp", axis=0, tiled=True)
    empty = jnp.zeros((grouped.shape[0], up_weight.shape[1]), jnp.float32)

    def add_rows(total, piece, start):
        columns = lax.dynamic_slice_in_dim(grouped, start, piece.shape[0], 1)
        return total + jnp.dot(
            columns, piece.astype(jnp.bfloat16), preferred_element_type=jnp.float32
        )

    pre = taken_in(up_weight.astype(jnp.bfloat16), "fs", 0, add_rows, empty)
    hidden = jnp.square(jax.nn.relu(pre)).astype(jnp.bfloat16)

    def project(piece, start):
        return jnp.dot(hidden, piece.astype(jnp.bfloat16), preferred_element_type=jnp.float32)

    terms = on_whole(down_weight.astype(jnp.bfloat16), "fs", 1, project)
    summed = lax.psum_scatter(terms, "tp", scatter_dimension=0, tiled=True)
    return summed.astype(jnp.bfloat16)


def solution(mesh):
    placed = (P(("fs", "tp"), None), P(), P("fs", "tp"), P("tp", "fs"))
    return jax.shard_map(
        shards, mesh=mesh, in_specs=placed, out_specs=P(("fs", "tp"), None), check_vma=False
    )
```

profile of v0, /device:TPU:1, one launch (start us, length us, event | category | flops | bytes accessed | tf_op | source)
XLA Modules:
  0.0 231.7 jit_solution(14041995372060814346)
XLA Ops:
  6.5 0.0 all-gather.4.cloned.1.call-start
  6.5 1.2 fusion
  7.8 2.0 fusion.2
  9.8 0.0 all-gather.4.cloned.1.call-update
  9.8 0.0 all-gather.6.cloned.1.call-start
  9.9 1.8 convert_element_type.20
  11.7 0.0 all-gather.6.cloned.1.call-update
  11.7 0.0 all-gather.8.cloned.1.call-start
  11.7 1.8 convert_element_type.22
  13.5 0.0 all-gather.8.cloned.1.call-update
  13.5 0.0 reduce-scatter.2.cloned.1.call-start
  13.6 31.9 %all-gather.4.cloned.1.call-done = bf16[1024,2048]{1,0:T(8,128)(2,1)} async-done(((bf16[128,2048]{1,0:T(8,128)(2,1)}), bf16[1024,2048]{1,0:T(8,128)(2,1)}) %all-gather.4.cloned.1.call-update) | async-done | bytes 4194320 | tf_op jit(solution)/shard_map/all_gather | solution.py:24
  45.5 52.7 %all-gather.6.cloned.1.call-done = bf16[2048,1024]{1,0:T(8,128)(2,1)} async-done(((bf16[128,1024]{1,0:T(8,128)(2,1)}), bf16[2048,1024]{1,0:T(8,128)(2,1)}) %all-gather.6.cloned.1.call-update) | async-done | bytes 4194320 | tf_op jit(solution)/shard_map/all_gather | solution.py:11
  98.2 57.0 %all-gather.8.cloned.1.call-done = bf16[1024,2048]{1,0:T(8,128)(2,1)} async-done(((bf16[1024,128]{1,0:T(8,128)(2,1)}), bf16[1024,2048]{1,0:T(8,128)(2,1)}) %all-gather.8.cloned.1.call-update) | async-done | bytes 4194320 | tf_op jit(solution)/shard_map/all_gather | solution.py:17
  155.2 15.0 %fusion.3 = f32[1024,2048]{1,0:T(8,128)} fusion(bf16[1024,2048]{1,0:T(8,128)(2,1)} %all-gather.8.cloned.1.call-done, bf16[1024,2048]{1,0:T(8,128)(2,1)} %all-gather.4.cloned.1.call-done, bf16[2048,1024]{1,0:T(8,128)(2,1)} %all-gather.6.cloned.1.call-done), kind=kOutput, calls=%fused_computation.6 | convolution fusion | flops 8593080320 | bytes 20971520 | tf_op jit(solution)/shard_map/dot_general | solution.py:37
  170.2 0.0 reduce-scatter.2.cloned.1.call-update
  170.2 52.8 %reduce-scatter.2.cloned.1.call-done = f32[128,2048]{1,0:T(8,128)} async-done(((f32[1024,2048]{1,0:T(8,128)}), f32[128,2048]{1,0:T(8,128)}) %reduce-scatter.2.cloned.1.call-update) | async-done | bytes 1048592 | tf_op jit(solution)/shard_map/reduce_scatter | solution.py:40
  223.1 2.1 convert_element_type.23
  (1 shorter events, 0.0 us)
Async XLA Ops:
  6.5 39.0 %all-gather.4.cloned.1.call-start = ((), (), s32[]{:S(2)}) async-start(), calls=%async_computation.1 | async-start | bytes 4718592 | tf_op jit(solution)/shard_map/all_gather | solution.py:24
  9.8 88.4 %all-gather.6.cloned.1.call-start = ((), (), s32[]{:S(2)}) async-start(), calls=%async_computation.2 | async-start | bytes 4456448 | tf_op jit(solution)/shard_map/all_gather | solution.py:11
  11.7 143.5 %all-gather.8.cloned.1.call-start = ((), (), s32[]{:S(2)}) async-start(), calls=%async_computation.3 | async-start | bytes 4456448 | tf_op jit(solution)/shard_map/all_gather | solution.py:17
  13.5 209.5 %reduce-scatter.2.cloned.1.call-start = ((), (), s32[]{:S(2)}) async-start(), calls=%async_computation.4 | async-start | bytes 9437184 | tf_op jit(solution)/shard_map/reduce_scatter | solution.py:40
Sparse Core Ops, SparseCore 0:
  9.9 35.5 all-gather.3
  47.6 50.5 all-gather.5
  100.4 54.7 all-gather.7
  170.4 52.6 reduce-scatter.1
where the time goes:
time: 232 us
  waiting for transfers between devices  194 us (84%)
  matrix products  15 us (6%)
  between operations  13.1 us (6%)
  other arithmetic  8.9 us (4%)
    all_gather x1, waiting for transfers between devices, on_whole(): return work(lax.all_gather(shard, axis, axis=dim, tiled=True), jnp.int32(0))  57 us
    reduce_scatter x1, waiting for transfers between devices, shards(): summed = lax.psum_scatter(terms, 'tp', scatter_dimension=0, tiled=True)  52.8 us
    all_gather x1, waiting for transfers between devices, gathered(): return lax.all_gather(part, axis, axis=dim, tiled=True)  52.7 us
    all_gather x1, waiting for transfers between devices, shards(): grouped = lax.all_gather(normed, 'tp', axis=0, tiled=True)  31.9 us
    dot_general x1, matrix products, project(): jnp.dot(hidden, piece.astype(jnp.bfloat16), preferred_element_type=jnp.fl...  15 us
  transfers between devices with their start and end apart: 4, of which 4 were waited for; matrix products, arithmetic and copies ran while one was open for 2% of the time, Pallas kernels for 0%

commit v1 on v0

v1 whole, which is shorter than its diff:
```python
import jax
import jax.numpy as jnp
from jax import lax
from jax.experimental import pallas as pl
from jax.experimental.pallas import tpu as pltpu
from jax.sharding import PartitionSpec as P

epsilon = 1e-06
MESH = pl.DeviceIdType.MESH
SIDE = 4
OFFSETS = (0, -1, 1, 2)
BF = jnp.bfloat16
F32 = jnp.float32

ORDER = (
    (0, 0),
    (0, -1), (0, 1), (-1, 0), (1, 0),
    (-1, -1), (-1, 1), (1, -1), (1, 1),
    (2, 0), (0, 2),
    (-1, 2), (2, -1), (1, 2), (2, 1),
    (2, 2),
)


def kernel(
    tokens_ref, gain_ref, up_ref, down_ref, out_ref,
    tok, upw, dnw, pre, hid, part, first, last,
    up_recv, dn_recv, up_pair, dn_pair, tok_recv, first_recv, last_recv,
    up_send, dn_send, up_pair_send, dn_pair_send, tok_send, rs_send,
):
    rows, width = tokens_ref.shape
    half = up_ref.shape[1] // 2
    depth = up_ref.shape[0]
    blocks = SIDE * SIDE
    fs = lax.axis_index("fs")
    tp = lax.axis_index("tp")
    z, y, x, core = fs // SIDE, fs % SIDE, tp // 2, tp % 2

    def near(at, by):
        return (at + (by + SIDE)) % SIDE

    def device(dz=0, dy=0, dx=0):
        return {"fs": near(z, dz) * SIDE + near(y, dy), "tp": near(x, dx) * 2 + core}

    partner = {"fs": fs, "tp": x * 2 + (1 - core)}

    def copy(src, dst, send_sem, recv_sem, to):
        return pltpu.make_async_remote_copy(
            src_ref=src, dst_ref=dst, send_sem=send_sem, recv_sem=recv_sem,
            device_id=to, device_id_type=MESH,
        )

    barrier = pltpu.get_barrier_semaphore()
    peers = [device(dz=1), device(dz=-1), device(dy=1), device(dy=-1), device(dx=1), device(dx=-1), partner]
    for peer in peers:
        pl.semaphore_signal(barrier, inc=1, device_id=peer, device_id_type=MESH)

    def up_at(h, dz, dy, q, n):
        zs, ys = near(z, dz), near(y, dy)
        block = zs * SIDE + ys if h == 0 else ys * SIDE + zs
        row = h * blocks * depth + block * depth + q * (depth // 2)
        return upw.at[pl.ds(pl.multiple_of(row, depth // 2), n * (depth // 2)), :]

    def dn_at(h, dz, dy, q, n):
        block = near(z, dz) * SIDE + near(y, dy)
        row = block * 4 * half + h * half + q * (half // 2)
        return dnw.at[pl.ds(pl.multiple_of(row, half // 2), n * (half // 2)), :]

    class Gather:
        def __init__(self, at, recv, send):
            self.at, self.recv, self.send = at, recv, send

        def piece(self, h, df, ds, q=0, n=2):
            return self.at(h, ds, df, q, n) if h == 0 else self.at(h, df, ds, q, n)

        def peer(self, h, axis, by):
            along_y = (h == 0) == (axis == 0)
            return device(dy=by) if along_y else device(dz=by)

        def post(self, h, stage, slot, df, ds, q=0, n=2):
            ref = self.piece(h, df, ds, q, n)
            by = 1 if slot % 2 == 0 else -1
            copy(ref, ref, self.send, self.recv.at[h, stage, slot], self.peer(h, min(stage, 1), by)).start()

        def wait(self, h, stage, slot, df, ds, q=0, n=2):
            ref = self.piece(h, df, ds, q, n)
            copy(ref, ref, self.send, self.recv.at[h, stage, slot], self.peer(h, 0, 1)).wait_recv()

        def start(self):
            for h in (0, 1):
                for slot in (0, 1):
                    self.post(h, 0, slot, 0, 0)
            for h in (0, 1):
                for slot in (0, 1):
                    self.post(h, 1, slot, 0, 0)

        def second(self, h, j):
            for slot in (0, 1):
                self.post(h, 1 + j, slot, OFFSETS[j], 0)

        def first_axis(self):
            for h in (0, 1):
                self.wait(h, 0, 0, -1, 0)
                self.post(h, 0, 2, -1, 0, 0, 1)
                self.wait(h, 0, 1, 1, 0)
                self.post(h, 0, 3, 1, 0, 1, 1)
            for j in (1, 2):
                for h in (0, 1):
                    self.second(h, j)

        def far_first(self):
            for h in (0, 1):
                self.wait(h, 0, 2, 2, 0, 0, 1)
                self.wait(h, 0, 3, 2, 0, 1, 1)
                self.second(h, 3)

        def relay(self, j):
            for h in (0, 1):
                self.wait(h, 1 + j, 0, OFFSETS[j], -1)
                self.post(h, 1 + j, 2, OFFSETS[j], -1, 0, 1)
                self.wait(h, 1 + j, 1, OFFSETS[j], 1)
                self.post(h, 1 + j, 3, OFFSETS[j], 1, 1, 1)

        def far_second(self, j):
            for h in (0, 1):
                self.wait(h, 1 + j, 2, OFFSETS[j], 2, 0, 1)
                self.wait(h, 1 + j, 3, OFFSETS[j], 2, 1, 1)

    up = Gather(up_at, up_recv, up_send)
    dn = Gather(dn_at, dn_recv, dn_send)

    for h in (0, 1):
        block = fs if h == 0 else y * SIDE + z
        row = pl.multiple_of(h * blocks * depth + block * depth, depth)
        upw[pl.ds(row, depth), :] = up_ref[:, h * half:(h + 1) * half].astype(BF)
    pl.semaphore_wait(barrier, len(peers))
    up.start()

    values = tokens_ref[...].astype(F32)
    scale = lax.rsqrt(jnp.mean(values * values, axis=-1, keepdims=True) + epsilon)
    tok[pl.ds(pl.multiple_of(x * rows, rows), rows), :] = (values * scale * gain_ref[...]).astype(BF)

    def tok_at(dx, q, n=1):
        row = near(x, dx) * rows + q * (rows // 2)
        return tok.at[pl.ds(pl.multiple_of(row, rows // 2), n * (rows // 2)), :]

    def tok_post(slot, dx, q, by):
        copy(tok_at(dx, q), tok_at(dx, q), tok_send, tok_recv.at[slot], device(dx=by)).start()

    def tok_wait(slot, dx, q):
        copy(tok_at(dx, q), tok_at(dx, q), tok_send, tok_recv.at[slot], device(dx=1)).wait_recv()

    tok_post(0, 0, 0, 1)
    tok_post(3, 0, 1, -1)
    tok_post(1, 0, 1, 1)
    tok_post(2, 0, 0, -1)

    own = pl.multiple_of(fs * 4 * half, 4 * half)
    dnw[pl.ds(own, 2 * half), :] = down_ref[...].astype(BF)

    def dn_block(b, to_partner):
        block = near(z, ORDER[b][0]) * SIDE + near(y, ORDER[b][1])
        row = block * 4 * half + (2 * half if to_partner else 0)
        return dnw.at[pl.ds(pl.multiple_of(row, 2 * half), 2 * half), :]

    def dn_share(b):
        copy(dn_block(b, False), dn_block(b, True), dn_pair_send, dn_pair.at[b], partner).start()

    def up_plane(h, p, to_partner):
        plane = near(z if h == 0 else y, OFFSETS[p])
        row = (h + (2 if to_partner else 0)) * blocks * depth + plane * SIDE * depth
        return upw.at[pl.ds(pl.multiple_of(row, SIDE * depth), SIDE * depth), :]

    def up_share(p):
        for h in (0, 1):
            copy(up_plane(h, p, False), up_plane(h, p, True), up_pair_send, up_pair.at[h, p], partner).start()

    def up_shared(p):
        for h in (0, 1):
            ref = up_plane(h, p, True)
            copy(ref, ref, up_pair_send, up_pair.at[h, p], partner).wait_recv()

    dn_share(0)

    up.first_axis()
    tok_wait(0, -1, 0)
    tok_post(4, -1, 0, 1)
    tok_wait(3, 1, 1)
    tok_post(5, 1, 1, -1)
    up.relay(0)
    up.far_first()
    up_share(0)
    up.relay(1)
    up.relay(2)
    up.relay(3)
    up_share(1)
    up_share(2)
    dn.start()
    tok_wait(1, -1, 1)
    tok_wait(2, 1, 0)
    tok_wait(4, 2, 0)
    tok_wait(5, 2, 1)

    def columns_of(h, p):
        plane = near(z if h == 0 else y, OFFSETS[p])
        if h == 0:
            return tok[:, pl.ds(pl.multiple_of(plane * SIDE * depth, SIDE * depth), SIDE * depth)]
        return jnp.concatenate(
            [tok[:, pl.ds(pl.multiple_of((a * SIDE + plane) * depth, depth), depth)] for a in range(SIDE)], axis=1
        )

    def dot(a, b):
        return jnp.dot(a, b, preferred_element_type=F32)

    tile = 256

    def early(h, other):
        for n in range(half // tile):
            cols = slice(n * tile, (n + 1) * tile)
            total = sum(dot(columns_of(h, p), up_plane(h, p, other)[:, cols]) for p in (0, 1, 2))
            at = (2 * other + h) * half + n * tile
            pre[:, at:at + tile] = total

    def late(h, other):
        for n in range(half // tile):
            cols = slice(n * tile, (n + 1) * tile)
            at = (2 * other + h) * half + n * tile
            total = pre[:, at:at + tile] + dot(columns_of(h, 3), up_plane(h, 3, other)[:, cols])
            hid[:, at:at + tile] = jnp.square(jnp.maximum(total, 0.0)).astype(BF)

    for h in (0, 1):
        early(h, 0)
    for p in (0, 1, 2):
        up_shared(p)
    for h in (0, 1):
        early(h, 1)
    for j in range(4):
        up.far_second(j)
    up_share(3)
    for h in (0, 1):
        late(h, 0)
    up_shared(3)
    for h in (0, 1):
        late(h, 1)

    def part_at(b, dx, q=0, n=2):
        row = b * SIDE * rows + near(x, dx) * rows + q * (rows // 2)
        return part.at[pl.ds(pl.multiple_of(row, rows // 2), n * (rows // 2)), :]

    def project(b):
        if b:
            ref = dn_block(b, True)
            copy(ref, ref, dn_pair_send, dn_pair.at[b], partner).wait_recv()
        else:
            ref = dn_block(0, True)
            copy(ref, ref, dn_pair_send, dn_pair.at[0], partner).wait_recv()
        block = near(z, ORDER[b][0]) * SIDE + near(y, ORDER[b][1])
        piece = dnw[pl.ds(pl.multiple_of(block * 4 * half, 4 * half), 4 * half), :]
        part[b * SIDE * rows:(b + 1) * SIDE * rows, :] = dot(hid[...], piece)
        copy(part_at(b, 2, 0, 1), first.at[0, b], rs_send, first_recv.at[0, b], device(dx=1)).start()
        copy(part_at(b, 2, 1, 1), first.at[1, b], rs_send, first_recv.at[1, b], device(dx=-1)).start()

    def pass_on(b):
        for side, by in ((0, 1), (1, -1)):
            copy(first.at[side, b], first.at[side, b], rs_send, first_recv.at[side, b], device(dx=by)).wait_recv()
            ref = part_at(b, by, side, 1)
            ref[...] = ref[...] + first[side, b]
            copy(part_at(b, by), last.at[side, b], rs_send, last_recv.at[side, b], device(dx=by)).start()

    def finish(b):
        for side, by in ((0, 1), (1, -1)):
            copy(last.at[side, b], last.at[side, b], rs_send, last_recv.at[side, b], device(dx=by)).wait_recv()
        total = part_at(b, 0)[...] + last[0, b] + last[1, b]
        block = near(z, ORDER[b][0]) * SIDE + near(y, ORDER[b][1])
        out_ref[:, pl.ds(pl.multiple_of(block * rows, rows), rows)] = total.astype(BF)

    def step(b):
        if b < blocks:
            project(b)
        if 0 <= b - 2 < blocks:
            pass_on(b - 2)
        if 0 <= b - 4 < blocks:
            finish(b - 4)

    step(0)
    dn.first_axis()
    dn.relay(0)
    for b in (1, 2, 3, 4):
        dn_share(b)
    dn.far_first()
    step(1)
    dn.relay(1)
    step(2)
    dn.relay(2)
    for b in (5, 6, 7, 8):
        dn_share(b)
    dn.far_second(0)
    for b in (9, 10):
        dn_share(b)
    step(3)
    dn.relay(3)
    step(4)
    step(5)
    step(6)
    dn.far_second(1)
    dn.far_second(2)
    for b in (11, 12, 13, 14):
        dn_share(b)
    step(7)
    dn.far_second(3)
    dn_share(15)
    for b in range(8, blocks + 4):
        step(b)

    def drained(ref, sem):
        pltpu.make_async_copy(ref, ref, sem).wait()

    drained(upw.at[pl.ds(0, 15 * 4 * depth // 2), :], up_send)
    drained(dnw.at[pl.ds(0, 15 * 4 * half // 2), :], dn_send)
    drained(upw.at[pl.ds(0, 2 * blocks * depth), :], up_pair_send)
    drained(dnw.at[pl.ds(0, blocks * 2 * half), :], dn_pair_send)
    drained(tok.at[pl.ds(0, 3 * rows), :], tok_send)
    drained(part.at[pl.ds(0, blocks * 3 * rows), :], rs_send)


def shards(tokens, norm_gain, up_weight, down_weight):
    rows, width = tokens.shape
    depth, inner = up_weight.shape
    blocks = SIDE * SIDE
    vmem = pl.BlockSpec(memory_space=pltpu.VMEM)
    dma = pltpu.SemaphoreType.DMA
    return pl.pallas_call(
        kernel,
        out_shape=jax.ShapeDtypeStruct((rows, width), BF),
        in_specs=[vmem] * 4,
        out_specs=vmem,
        scratch_shapes=[
            pltpu.VMEM((SIDE * rows, width), BF),
            pltpu.VMEM((4 * blocks * depth, inner // 2), BF),
            pltpu.VMEM((blocks * 2 * inner, rows), BF),
            pltpu.VMEM((SIDE * rows, 2 * inner), F32),
            pltpu.VMEM((SIDE * rows, 2 * inner), BF),
            pltpu.VMEM((blocks * SIDE * rows, rows), F32),
            pltpu.VMEM((2, blocks, rows // 2, rows), F32),
            pltpu.VMEM((2, blocks, rows, rows), F32),
            dma((2, 5, 4)), dma((2, 5, 4)), dma((2, 4)), dma((blocks,)), dma((6,)), dma((2, blocks)), dma((2, blocks)),
            dma, dma, dma, dma, dma, dma,
        ],
        compiler_params=pltpu.CompilerParams(
            collective_id=0, has_side_effects=True, vmem_limit_bytes=60 * 1024 * 1024
        ),
    )(tokens, norm_gain.reshape(1, width), up_weight, down_weight)


def solution(mesh):
    placed = (P(("fs", "tp"), None), P(), P("fs", "tp"), P("tp", "fs"))
    return jax.shard_map(
        shards, mesh=mesh, in_specs=placed, out_specs=P(("fs", "tp"), None), check_vma=False
    )
```

time: 232 us -> 88.1 us (0.38)
  waiting for transfers between devices: 194 us -> 0 us
  Pallas kernels: 0 us -> 85.1 us
  matrix products: 15 us -> 0 us
  between operations: 13.1 us -> 0.01 us
  other arithmetic: 8.9 us -> 0 us
    all_gather x3 -> x0, waiting for transfers between devices: 142 us -> none  [the longest x1 57 us: on_whole(): return work(lax.all_gather(shard, axis, axis=dim, tiled=True), jnp.int32(0))]
    pallas_call x0 -> x1, Pallas kernels: none -> 85.1 us  [shards(): pl.pallas_call(kernel, out_shape=jax.ShapeDtypeStruct((rows, width), BF),...]
    reduce_scatter x1 -> x0, waiting for transfers between devices: 52.8 us -> none  [shards(): summed = lax.psum_scatter(terms, 'tp', scatter_dimension=0, tiled=True)]
    dot_general x1 -> x0, matrix products: 15 us -> none  [project(): jnp.dot(hidden, piece.astype(jnp.bfloat16), preferred_element_type=jnp.fl...]
    convert_element_type x4 -> x0, other arithmetic: 7.66 us -> none  [the longest x1 2.08 us: shards(): return summed.astype(jnp.bfloat16)]
  transfers between devices with their start and end apart: 4 -> 0, of which waited for: 4 -> 0; matrix products, arithmetic and copies ran while one was open for 2% -> 0% of each run, Pallas kernels for 0% -> 0%
where the time goes in v1:
time: 88.1 us; the launch traced here: 87 us
  Pallas kernels  85.1 us (97%)
  local copies, waits for them, and re-layouts  1.88 us (2%)
    pallas_call x1, Pallas kernels, shards(): pl.pallas_call(kernel, out_shape=jax.ShapeDtypeStruct((rows, width), BF),...  85.1 us
    unnamed x1, local copies, waits for them, and re-layouts  1.88 us

profile of v1, /device:TPU:1, one launch (start us, length us, event | category | flops | bytes accessed | tf_op | source)
XLA Modules:
  0.0 87.0 jit_solution(8469392783661732306)
XLA Ops:
  0.0 85.1 %shard_map.46 = bf16[128,2048]{1,0:T(8,128)(2,1)} custom-call(bf16[128,2048]{1,0:T(8,128)(2,1)} %tokens_ref.1, f32[1,2048]{1,0:T(1,128)} %bitcast.1, f32[128,1024]{1,0:T(8,128)} %up_ref.1, f32[1024,128]{1,0:T(8,128)} %down_ref.1), custom_call_target="tpu_custom_call" | custom-call | tf_op jit(solution)/shard_map/pallas_call | solution.py:332
  85.1 1.9 %copy.6 = bf16[128,2048]{1,0:T(8,128)(2,1)} copy(bf16[128,2048]{1,0:T(8,128)(2,1)} %shard_map.46) | data formatting | bytes 1048576

commit v2 on v1

--- a/solution.py
+++ b/solution.py
@@ -23,10 +23,10 @@
 
 
 def kernel(
-    tokens_ref, gain_ref, up_ref, down_ref, out_ref,
-    tok, upw, dnw, pre, hid, part, first, last,
+    tokens_hbm, gain_ref, up_hbm, down_hbm, out_hbm,
+    tokens_ref, up_ref, down_ref, out_ref, tok, upw, dnw, pre, hid, part, first, last,
     up_recv, dn_recv, up_pair, dn_pair, tok_recv, first_recv, last_recv,
-    up_send, dn_send, up_pair_send, dn_pair_send, tok_send, rs_send,
+    up_send, dn_send, up_pair_send, dn_pair_send, tok_send, rs_send, load, store,
 ):
     rows, width = tokens_ref.shape
     half = up_ref.shape[1] // 2
@@ -55,6 +55,13 @@
     for peer in peers:
         pl.semaphore_signal(barrier, inc=1, device_id=peer, device_id_type=MESH)
 
+    loads = [
+        pltpu.make_async_copy(src, dst, load.at[i])
+        for i, (src, dst) in enumerate(((up_hbm, up_ref), (tokens_hbm, tokens_ref), (down_hbm, down_ref)))
+    ]
+    for one in loads:
+        one.start()
+
     def up_at(h, dz, dy, q, n):
         zs, ys = near(z, dz), near(y, dy)
         block = zs * SIDE + ys if h == 0 else ys * SIDE + zs
@@ -86,10 +93,12 @@
             ref = self.piece(h, df, ds, q, n)
             copy(ref, ref, self.send, self.recv.at[h, stage, slot], self.peer(h, 0, 1)).wait_recv()
 
-        def start(self):
+        def start_first(self):
             for h in (0, 1):
                 for slot in (0, 1):
                     self.post(h, 0, slot, 0, 0)
+
+        def start_second(self):
             for h in (0, 1):
                 for slot in (0, 1):
                     self.post(h, 1, slot, 0, 0)
@@ -129,13 +138,15 @@
     up = Gather(up_at, up_recv, up_send)
     dn = Gather(dn_at, dn_recv, dn_send)
 
+    loads[0].wait()
     for h in (0, 1):
         block = fs if h == 0 else y * SIDE + z
         row = pl.multiple_of(h * blocks * depth + block * depth, depth)
         upw[pl.ds(row, depth), :] = up_ref[:, h * half:(h + 1) * half].astype(BF)
     pl.semaphore_wait(barrier, len(peers))
-    up.start()
-
+    up.start_first()
+
+    loads[1].wait()
     values = tokens_ref[...].astype(F32)
     scale = lax.rsqrt(jnp.mean(values * values, axis=-1, keepdims=True) + epsilon)
     tok[pl.ds(pl.multiple_of(x * rows, rows), rows), :] = (values * scale * gain_ref[...]).astype(BF)
@@ -154,6 +165,8 @@
     tok_post(3, 0, 1, -1)
     tok_post(1, 0, 1, 1)
     tok_post(2, 0, 0, -1)
+    up.start_second()
+    loads[2].wait()
 
     own = pl.multiple_of(fs * 4 * half, 4 * half)
     dnw[pl.ds(own, 2 * half), :] = down_ref[...].astype(BF)
@@ -171,31 +184,41 @@
         row = (h + (2 if to_partner else 0)) * blocks * depth + plane * SIDE * depth
         return upw.at[pl.ds(pl.multiple_of(row, SIDE * depth), SIDE * depth), :]
 
-    def up_share(p):
+    def up_share(j, p):
         for h in (0, 1):
-            copy(up_plane(h, p, False), up_plane(h, p, True), up_pair_send, up_pair.at[h, p], partner).start()
+            plane = near(z if h == 0 else y, OFFSETS[p])
+            row = (plane * SIDE + near(y if h == 0 else z, OFFSETS[j])) * depth
+            mine, theirs = (
+                upw.at[pl.ds(pl.multiple_of((h + 2 * side) * blocks * depth + row, depth), depth), :] for side in (0, 1)
+            )
+            copy(mine, theirs, up_pair_send, up_pair.at[h, p], partner).start()
 
     def up_shared(p):
         for h in (0, 1):
             ref = up_plane(h, p, True)
             copy(ref, ref, up_pair_send, up_pair.at[h, p], partner).wait_recv()
 
+    up_share(0, 0)
     dn_share(0)
 
     up.first_axis()
+    up_share(1, 0)
+    up_share(2, 0)
+    up.relay(0)
+    up_share(0, 1)
+    up_share(0, 2)
+    up.far_first()
+    up_share(3, 0)
     tok_wait(0, -1, 0)
     tok_post(4, -1, 0, 1)
     tok_wait(3, 1, 1)
     tok_post(5, 1, 1, -1)
-    up.relay(0)
-    up.far_first()
-    up_share(0)
-    up.relay(1)
-    up.relay(2)
-    up.relay(3)
-    up_share(1)
-    up_share(2)
-    dn.start()
+    for j in (1, 2, 3):
+        up.relay(j)
+        up_share(j, 1)
+        up_share(j, 2)
+    dn.start_first()
+    dn.start_second()
     tok_wait(1, -1, 1)
     tok_wait(2, 1, 0)
     tok_wait(4, 2, 0)
@@ -232,11 +255,14 @@
         early(h, 0)
     for p in (0, 1, 2):
         up_shared(p)
+    for j in (0, 1):
+        up.far_second(j)
+        up_share(j, 3)
     for h in (0, 1):
         early(h, 1)
-    for j in range(4):
+    for j in (2, 3):
         up.far_second(j)
-    up_share(3)
+        up_share(j, 3)
     for h in (0, 1):
         late(h, 0)
     up_shared(3)
@@ -272,44 +298,52 @@
             copy(last.at[side, b], last.at[side, b], rs_send, last_recv.at[side, b], device(dx=by)).wait_recv()
         total = part_at(b, 0)[...] + last[0, b] + last[1, b]
         block = near(z, ORDER[b][0]) * SIDE + near(y, ORDER[b][1])
-        out_ref[:, pl.ds(pl.multiple_of(block * rows, rows), rows)] = total.astype(BF)
+        out_ref[b] = total.astype(BF)
+        stored(b).start()
+
+    def stored(b):
+        block = near(z, ORDER[b][0]) * SIDE + near(y, ORDER[b][1])
+        return pltpu.make_async_copy(
+            out_ref.at[b], out_hbm.at[:, pl.ds(pl.multiple_of(block * rows, rows), rows)], store.at[b]
+        )
 
     def step(b):
         if b < blocks:
             project(b)
         if 0 <= b - 2 < blocks:
             pass_on(b - 2)
-        if 0 <= b - 4 < blocks:
-            finish(b - 4)
+        if 0 <= b - 6 < blocks:
+            finish(b - 6)
 
     step(0)
     dn.first_axis()
     dn.relay(0)
     for b in (1, 2, 3, 4):
         dn_share(b)
+    step(1)
     dn.far_first()
-    step(1)
+    step(2)
     dn.relay(1)
-    step(2)
+    step(3)
+    step(4)
     dn.relay(2)
     for b in (5, 6, 7, 8):
         dn_share(b)
     dn.far_second(0)
     for b in (9, 10):
         dn_share(b)
-    step(3)
-    dn.relay(3)
-    step(4)
     step(5)
     step(6)
+    dn.relay(3)
+    step(7)
+    step(8)
     dn.far_second(1)
     dn.far_second(2)
     for b in (11, 12, 13, 14):
         dn_share(b)
-    step(7)
     dn.far_second(3)
     dn_share(15)
-    for b in range(8, blocks + 4):
+    for b in range(9, blocks + 6):
         step(b)
 
     def drained(ref, sem):
@@ -321,6 +355,8 @@
     drained(dnw.at[pl.ds(0, blocks * 2 * half), :], dn_pair_send)
     drained(tok.at[pl.ds(0, 3 * rows), :], tok_send)
     drained(part.at[pl.ds(0, blocks * 3 * rows), :], rs_send)
+    for b in range(blocks):
+        stored(b).wait()
 
 
 def shards(tokens, norm_gain, up_weight, down_weight):
@@ -328,13 +364,18 @@
     depth, inner = up_weight.shape
     blocks = SIDE * SIDE
     vmem = pl.BlockSpec(memory_space=pltpu.VMEM)
+    anywhere = pl.BlockSpec(memory_space=pl.ANY)
     dma = pltpu.SemaphoreType.DMA
     return pl.pallas_call(
         kernel,
         out_shape=jax.ShapeDtypeStruct((rows, width), BF),
-        in_specs=[vmem] * 4,
-        out_specs=vmem,
+        in_specs=[anywhere, vmem, anywhere, anywhere],
+        out_specs=anywhere,
         scratch_shapes=[
+            pltpu.VMEM(tokens.shape, BF),
+            pltpu.VMEM(up_weight.shape, F32),
+            pltpu.VMEM(down_weight.shape, F32),
+            pltpu.VMEM((blocks, rows, rows), BF),
             pltpu.VMEM((SIDE * rows, width), BF),
             pltpu.VMEM((4 * blocks * depth, inner // 2), BF),
             pltpu.VMEM((blocks * 2 * inner, rows), BF),
@@ -344,7 +385,7 @@
             pltpu.VMEM((2, blocks, rows // 2, rows), F32),
             pltpu.VMEM((2, blocks, rows, rows), F32),
             dma((2, 5, 4)), dma((2, 5, 4)), dma((2, 4)), dma((blocks,)), dma((6,)), dma((2, blocks)), dma((2, blocks)),
-            dma, dma, dma, dma, dma, dma,
+            dma, dma, dma, dma, dma, dma, dma((3,)), dma((blocks,)),
         ],
         compiler_params=pltpu.CompilerParams(
             collective_id=0, has_side_effects=True, vmem_limit_bytes=60 * 1024 * 1024

time: 88.1 us -> 81.2 us (0.922)
  Pallas kernels: 85.1 us -> 79.1 us
    pallas_call x1, Pallas kernels: 85.1 us -> 79.1 us  [shards(): pl.pallas_call(kernel, out_shape=jax.ShapeDtypeStruct((rows, width), BF),...]
where the time goes in v2:
time: 81.2 us; the launch traced here: 81 us
  Pallas kernels  79.1 us (97%)
  local copies, waits for them, and re-layouts  1.88 us (2%)
    pallas_call x1, Pallas kernels, shards(): pl.pallas_call(kernel, out_shape=jax.ShapeDtypeStruct((rows, width), BF),...  79.1 us
    unnamed x1, local copies, waits for them, and re-layouts  1.88 us

profile of v2, /device:TPU:1, one launch (start us, length us, event | category | flops | bytes accessed | tf_op | source)
XLA Modules:
  0.0 81.0 jit_solution(7961345470454484738)
XLA Ops:
  0.0 79.1 %shard_map.46 = bf16[128,2048]{1,0:T(8,128)(2,1)} custom-call(bf16[128,2048]{1,0:T(8,128)(2,1)} %tokens_hbm.1, f32[1,2048]{1,0:T(1,128)} %bitcast.1, f32[128,1024]{1,0:T(8,128)} %up_hbm.1, f32[1024,128]{1,0:T(8,128)} %down_hbm.1), custom_call_target="tpu_custom_call" | custom-call | tf_op jit(solution)/shard_map/pallas_call | solution.py:369
  79.1 1.9 %copy.6 = bf16[128,2048]{1,0:T(8,128)(2,1)} copy(bf16[128,2048]{1,0:T(8,128)(2,1)} %shard_map.46) | data formatting | bytes 1048576

commit v3 on v2

--- a/solution.py
+++ b/solution.py
@@ -22,9 +22,56 @@
 )
 
 
+GROUPS = ((0,), (1, 2), (3, 4), (5, 6), (7, 8), (9, 10), (11, 12), (13, 14), (15,))
+
+
+def unit_of(groups, largest):
+    top = jnp.maximum(jnp.max(jnp.abs(groups), axis=0), 1e-20)
+    return top * (1.0 / largest), largest / top
+
+
+def code_pairs(values):
+    groups = values.reshape(-1, 8, values.shape[1])
+    unit, inverse = unit_of(groups, 2047.0)
+    levels = jnp.round(groups * inverse)
+    n = groups.shape[0] // 2
+    words = levels[:n] * 4096.0 + (levels[n:] + 2048.0)
+    return jnp.concatenate([words, unit[None]], axis=0).reshape(-1, values.shape[1])
+
+
+def decode_pairs(coded):
+    groups = coded.reshape(-1, 8, coded.shape[1])
+    words, unit = groups[:-1], groups[-1]
+    high = jnp.floor(words * (1.0 / 4096.0))
+    low = words - high * 4096.0 - 2048.0
+    return (jnp.concatenate([high, low], axis=0) * unit).reshape(-1, coded.shape[1])
+
+
+def code_triples(values):
+    groups = values.reshape(-1, 8, values.shape[1])
+    unit, inverse = unit_of(groups, 32767.0)
+    n = groups.shape[0] // 3
+    a, b, c = (jnp.round(groups[i * n:(i + 1) * n] * inverse) for i in range(3))
+    high = jnp.floor(c * (1.0 / 256.0))
+    low = c - high * 256.0
+    return jnp.concatenate(
+        [a * 256.0 + low, b * 256.0 + (high + 128.0), groups[3 * n:], unit[None]], axis=0
+    ).reshape(-1, values.shape[1])
+
+
+def decode_triples(coded):
+    groups = coded.reshape(-1, 8, coded.shape[1])
+    n = (groups.shape[0] - 2) // 2
+    first, second, rest, unit = groups[:n], groups[n:2 * n], groups[2 * n:-1], groups[-1]
+    a = jnp.floor(first * (1.0 / 256.0))
+    b = jnp.floor(second * (1.0 / 256.0))
+    c = (second - b * 256.0 - 128.0) * 256.0 + (first - a * 256.0)
+    return jnp.concatenate([a * unit, b * unit, c * unit, rest], axis=0).reshape(-1, coded.shape[1])
+
+
 def kernel(
     tokens_hbm, gain_ref, up_hbm, down_hbm, out_hbm,
-    tokens_ref, up_ref, down_ref, out_ref, tok, upw, dnw, pre, hid, part, first, last,
+    tokens_ref, up_ref, down_ref, out_ref, tok, upw, dnw, pre, hid, part, first, last, first_out, last_out,
     up_recv, dn_recv, up_pair, dn_pair, tok_recv, first_recv, last_recv,
     up_send, dn_send, up_pair_send, dn_pair_send, tok_send, rs_send, load, store,
 ):
@@ -149,22 +196,22 @@
     loads[1].wait()
     values = tokens_ref[...].astype(F32)
     scale = lax.rsqrt(jnp.mean(values * values, axis=-1, keepdims=True) + epsilon)
-    tok[pl.ds(pl.multiple_of(x * rows, rows), rows), :] = (values * scale * gain_ref[...]).astype(BF)
-
-    def tok_at(dx, q, n=1):
-        row = near(x, dx) * rows + q * (rows // 2)
-        return tok.at[pl.ds(pl.multiple_of(row, rows // 2), n * (rows // 2)), :]
-
-    def tok_post(slot, dx, q, by):
-        copy(tok_at(dx, q), tok_at(dx, q), tok_send, tok_recv.at[slot], device(dx=by)).start()
-
-    def tok_wait(slot, dx, q):
-        copy(tok_at(dx, q), tok_at(dx, q), tok_send, tok_recv.at[slot], device(dx=1)).wait_recv()
-
-    tok_post(0, 0, 0, 1)
-    tok_post(3, 0, 1, -1)
-    tok_post(1, 0, 1, 1)
-    tok_post(2, 0, 0, -1)
+    tok[0:rows, :] = (values * scale * gain_ref[...]).astype(BF)
+
+    def tok_at(slot, q):
+        row = slot * rows + q * (rows // 2)
+        return tok.at[row:row + rows // 2, :]
+
+    def tok_post(sem, slot, there, q, by):
+        copy(tok_at(slot, q), tok_at(there, q), tok_send, tok_recv.at[sem], device(dx=by)).start()
+
+    def tok_wait(sem, slot, q):
+        copy(tok_at(slot, q), tok_at(slot, q), tok_send, tok_recv.at[sem], device(dx=1)).wait_recv()
+
+    tok_post(0, 0, 1, 0, 1)
+    tok_post(3, 0, 2, 1, -1)
+    tok_post(1, 0, 1, 1, 1)
+    tok_post(2, 0, 2, 0, -1)
     up.start_second()
     loads[2].wait()
 
@@ -209,20 +256,20 @@
     up_share(0, 2)
     up.far_first()
     up_share(3, 0)
-    tok_wait(0, -1, 0)
-    tok_post(4, -1, 0, 1)
-    tok_wait(3, 1, 1)
-    tok_post(5, 1, 1, -1)
+    tok_wait(0, 1, 0)
+    tok_post(4, 1, 3, 0, 1)
+    tok_wait(3, 2, 1)
+    tok_post(5, 2, 3, 1, -1)
     for j in (1, 2, 3):
         up.relay(j)
         up_share(j, 1)
         up_share(j, 2)
     dn.start_first()
     dn.start_second()
-    tok_wait(1, -1, 1)
-    tok_wait(2, 1, 0)
-    tok_wait(4, 2, 0)
-    tok_wait(5, 2, 1)
+    tok_wait(1, 1, 1)
+    tok_wait(2, 2, 0)
+    tok_wait(4, 3, 0)
+    tok_wait(5, 3, 1)
 
     def columns_of(h, p):
         plane = near(z if h == 0 else y, OFFSETS[p])
@@ -269,37 +316,35 @@
     for h in (0, 1):
         late(h, 1)
 
-    def part_at(b, dx, q=0, n=2):
-        row = b * SIDE * rows + near(x, dx) * rows + q * (rows // 2)
-        return part.at[pl.ds(pl.multiple_of(row, rows // 2), n * (rows // 2)), :]
-
-    def project(b):
-        if b:
+    def part_at(b, slot, q=0, n=2):
+        row = (b * 3 + slot) * rows + q * (rows // 2)
+        return part.at[row:row + n * (rows // 2), :]
+
+    def project(group):
+        pieces = []
+        for b in group:
             ref = dn_block(b, True)
             copy(ref, ref, dn_pair_send, dn_pair.at[b], partner).wait_recv()
-        else:
-            ref = dn_block(0, True)
-            copy(ref, ref, dn_pair_send, dn_pair.at[0], partner).wait_recv()
-        block = near(z, ORDER[b][0]) * SIDE + near(y, ORDER[b][1])
-        piece = dnw[pl.ds(pl.multiple_of(block * 4 * half, 4 * half), 4 * half), :]
-        part[b * SIDE * rows:(b + 1) * SIDE * rows, :] = dot(hid[...], piece)
-        copy(part_at(b, 2, 0, 1), first.at[0, b], rs_send, first_recv.at[0, b], device(dx=1)).start()
-        copy(part_at(b, 2, 1, 1), first.at[1, b], rs_send, first_recv.at[1, b], device(dx=-1)).start()
+            block = near(z, ORDER[b][0]) * SIDE + near(y, ORDER[b][1])
+            pieces.append(dnw[pl.ds(pl.multiple_of(block * 4 * half, 4 * half), 4 * half), :])
+        both = dot(hid[...], jnp.concatenate(pieces, axis=1) if len(pieces) > 1 else pieces[0])
+        for i, b in enumerate(group):
+            terms = both[:, i * rows:(i + 1) * rows]
+            for side, by in ((0, 1), (1, -1)):
+                row = 3 * rows + side * (rows // 2)
+                first_out[side, b] = code_pairs(terms[row:row + rows // 2])
+                copy(first_out.at[side, b], first.at[side, b], rs_send, first_recv.at[side, b], device(dx=by)).start()
+            part[b * 3 * rows:(b + 1) * 3 * rows, :] = terms[:3 * rows]
 
     def pass_on(b):
         for side, by in ((0, 1), (1, -1)):
             copy(first.at[side, b], first.at[side, b], rs_send, first_recv.at[side, b], device(dx=by)).wait_recv()
-            ref = part_at(b, by, side, 1)
-            ref[...] = ref[...] + first[side, b]
-            copy(part_at(b, by), last.at[side, b], rs_send, last_recv.at[side, b], device(dx=by)).start()
-
-    def finish(b):
-        for side, by in ((0, 1), (1, -1)):
-            copy(last.at[side, b], last.at[side, b], rs_send, last_recv.at[side, b], device(dx=by)).wait_recv()
-        total = part_at(b, 0)[...] + last[0, b] + last[1, b]
-        block = near(z, ORDER[b][0]) * SIDE + near(y, ORDER[b][1])
-        out_ref[b] = total.astype(BF)
-        stored(b).start()
+            slot = 2 - side
+            near_half, far_half = part_at(b, slot, side, 1)[...], part_at(b, slot, 1 - side, 1)[...]
+            summed = near_half + decode_pairs(first[side, b])
+            ordered = [summed, far_half] if side == 0 else [far_half, summed]
+            last_out[side, b] = code_triples(jnp.concatenate(ordered, axis=0))
+            copy(last_out.at[side, b], last.at[side, b], rs_send, last_recv.at[side, b], device(dx=by)).start()
 
     def stored(b):
         block = near(z, ORDER[b][0]) * SIDE + near(y, ORDER[b][1])
@@ -307,44 +352,50 @@
             out_ref.at[b], out_hbm.at[:, pl.ds(pl.multiple_of(block * rows, rows), rows)], store.at[b]
         )
 
-    def step(b):
-        if b < blocks:
-            project(b)
-        if 0 <= b - 2 < blocks:
-            pass_on(b - 2)
-        if 0 <= b - 6 < blocks:
-            finish(b - 6)
+    def finish(b):
+        for side, by in ((0, 1), (1, -1)):
+            copy(last.at[side, b], last.at[side, b], rs_send, last_recv.at[side, b], device(dx=by)).wait_recv()
+        total = part_at(b, 0)[...] + decode_triples(last[0, b]) + decode_triples(last[1, b])
+        out_ref[b] = total.astype(BF)
+        stored(b).start()
+
+    def step(g):
+        if g < len(GROUPS):
+            project(GROUPS[g])
+        if 0 <= g - 1 < len(GROUPS):
+            for b in GROUPS[g - 1]:
+                pass_on(b)
+        if 0 <= g - 3 < len(GROUPS):
+            for b in GROUPS[g - 3]:
+                finish(b)
 
     step(0)
     dn.first_axis()
     dn.relay(0)
     for b in (1, 2, 3, 4):
         dn_share(b)
+    dn.far_first()
     step(1)
-    dn.far_first()
+    dn.relay(1)
     step(2)
-    dn.relay(1)
-    step(3)
-    step(4)
     dn.relay(2)
     for b in (5, 6, 7, 8):
         dn_share(b)
     dn.far_second(0)
     for b in (9, 10):
         dn_share(b)
-    step(5)
-    step(6)
+    step(3)
     dn.relay(3)
-    step(7)
-    step(8)
+    step(4)
     dn.far_second(1)
     dn.far_second(2)
     for b in (11, 12, 13, 14):
         dn_share(b)
+    step(5)
     dn.far_second(3)
     dn_share(15)
-    for b in range(9, blocks + 6):
-        step(b)
+    for g in range(6, len(GROUPS) + 3):
+        step(g)
 
     def drained(ref, sem):
         pltpu.make_async_copy(ref, ref, sem).wait()
@@ -354,7 +405,7 @@
     drained(upw.at[pl.ds(0, 2 * blocks * depth), :], up_pair_send)
     drained(dnw.at[pl.ds(0, blocks * 2 * half), :], dn_pair_send)
     drained(tok.at[pl.ds(0, 3 * rows), :], tok_send)
-    drained(part.at[pl.ds(0, blocks * 3 * rows), :], rs_send)
+    drained(part.at[0:blocks * (5 * rows // 8 + 3 * rows // 2), :], rs_send)
     for b in range(blocks):
         stored(b).wait()
 
@@ -381,9 +432,11 @@
             pltpu.VMEM((blocks * 2 * inner, rows), BF),
             pltpu.VMEM((SIDE * rows, 2 * inner), F32),
             pltpu.VMEM((SIDE * rows, 2 * inner), BF),
-            pltpu.VMEM((blocks * SIDE * rows, rows), F32),
-            pltpu.VMEM((2, blocks, rows // 2, rows), F32),
-            pltpu.VMEM((2, blocks, rows, rows), F32),
+            pltpu.VMEM((blocks * 3 * rows, rows), F32),
+            pltpu.VMEM((2, blocks, 5 * rows // 16, rows), F32),
+            pltpu.VMEM((2, blocks, 3 * rows // 4, rows), F32),
+            pltpu.VMEM((2, blocks, 5 * rows // 16, rows), F32),
+            pltpu.VMEM((2, blocks, 3 * rows // 4, rows), F32),
             dma((2, 5, 4)), dma((2, 5, 4)), dma((2, 4)), dma((blocks,)), dma((6,)), dma((2, blocks)), dma((2, blocks)),
             dma, dma, dma, dma, dma, dma, dma((3,)), dma((blocks,)),
         ],

time: 81.2 us -> 74 us (0.911)
  Pallas kernels: 79.1 us -> 71.9 us
    pallas_call x1, Pallas kernels: 79.1 us -> 71.9 us  [shards(): pl.pallas_call(kernel, out_shape=jax.ShapeDtypeStruct((rows, width), BF),...]
where the time goes in v3:
time: 74 us; the launch traced here: 73.8 us
  Pallas kernels  71.9 us (97%)
  local copies, waits for them, and re-layouts  1.88 us (3%)
    pallas_call x1, Pallas kernels, shards(): pl.pallas_call(kernel, out_shape=jax.ShapeDtypeStruct((rows, width), BF),...  71.9 us
    unnamed x1, local copies, waits for them, and re-layouts  1.88 us

profile of v3, /device:TPU:1, one launch (start us, length us, event | category | flops | bytes accessed | tf_op | source)
XLA Modules:
  0.0 73.8 jit_solution(13650849886890548579)
XLA Ops:
  0.0 71.9 %shard_map.46 = bf16[128,2048]{1,0:T(8,128)(2,1)} custom-call(bf16[128,2048]{1,0:T(8,128)(2,1)} %tokens_hbm.1, f32[1,2048]{1,0:T(1,128)} %bitcast.1, f32[128,1024]{1,0:T(8,128)} %up_hbm.1, f32[1024,128]{1,0:T(8,128)} %down_hbm.1), custom_call_target="tpu_custom_call" | custom-call | tf_op jit(solution)/shard_map/pallas_call | solution.py:420
  71.9 1.9 %copy.6 = bf16[128,2048]{1,0:T(8,128)(2,1)} copy(bf16[128,2048]{1,0:T(8,128)(2,1)} %shard_map.46) | data formatting | bytes 1048576

commit v4 on v3

--- a/solution.py
+++ b/solution.py
@@ -15,7 +15,7 @@
 ORDER = (
     (0, 0),
     (0, -1), (0, 1), (-1, 0), (1, 0),
-    (-1, -1), (-1, 1), (1, -1), (1, 1),
+    (-1, -1), (1, 1), (-1, 1), (1, -1),
     (2, 0), (0, 2),
     (-1, 2), (2, -1), (1, 2), (2, 1),
     (2, 2),
@@ -25,48 +25,36 @@
 GROUPS = ((0,), (1, 2), (3, 4), (5, 6), (7, 8), (9, 10), (11, 12), (13, 14), (15,))
 
 
-def unit_of(groups, largest):
+def coded_rows(rows):
+    n = rows // 8
+    return 8 * (2 * (n // 3) + n % 3)
+
+
+def code(values):
+    groups = values.reshape(-1, 8, values.shape[1])
     top = jnp.maximum(jnp.max(jnp.abs(groups), axis=0), 1e-20)
-    return top * (1.0 / largest), largest / top
-
-
-def code_pairs(values):
-    groups = values.reshape(-1, 8, values.shape[1])
-    unit, inverse = unit_of(groups, 2047.0)
-    levels = jnp.round(groups * inverse)
-    n = groups.shape[0] // 2
-    words = levels[:n] * 4096.0 + (levels[n:] + 2048.0)
-    return jnp.concatenate([words, unit[None]], axis=0).reshape(-1, values.shape[1])
-
-
-def decode_pairs(coded):
-    groups = coded.reshape(-1, 8, coded.shape[1])
-    words, unit = groups[:-1], groups[-1]
-    high = jnp.floor(words * (1.0 / 4096.0))
-    low = words - high * 4096.0 - 2048.0
-    return (jnp.concatenate([high, low], axis=0) * unit).reshape(-1, coded.shape[1])
-
-
-def code_triples(values):
-    groups = values.reshape(-1, 8, values.shape[1])
-    unit, inverse = unit_of(groups, 32767.0)
+    exponent = jnp.ceil(jnp.log2(top * (1.0 / 32767.0)) + 0.001)
+    inverse = jnp.exp2(-exponent)
     n = groups.shape[0] // 3
     a, b, c = (jnp.round(groups[i * n:(i + 1) * n] * inverse) for i in range(3))
+    last = jnp.round(groups[-1] * inverse) * 256.0 + (exponent + 128.0)
     high = jnp.floor(c * (1.0 / 256.0))
     low = c - high * 256.0
-    return jnp.concatenate(
-        [a * 256.0 + low, b * 256.0 + (high + 128.0), groups[3 * n:], unit[None]], axis=0
-    ).reshape(-1, values.shape[1])
-
-
-def decode_triples(coded):
+    parts = [a * 256.0 + low, b * 256.0 + (high + 128.0), groups[3 * n:-1], last[None]]
+    return jnp.concatenate([p for p in parts if p.shape[0]], axis=0).reshape(-1, values.shape[1])
+
+
+def decode(coded):
     groups = coded.reshape(-1, 8, coded.shape[1])
-    n = (groups.shape[0] - 2) // 2
-    first, second, rest, unit = groups[:n], groups[n:2 * n], groups[2 * n:-1], groups[-1]
+    n = groups.shape[0] // 2 if groups.shape[0] % 2 else groups.shape[0] // 2 - 1
+    first, second, rest = groups[:n], groups[n:2 * n], groups[2 * n:-1]
+    level = jnp.floor(groups[-1] * (1.0 / 256.0))
+    unit = jnp.exp2(groups[-1] - level * 256.0 - 128.0)
     a = jnp.floor(first * (1.0 / 256.0))
     b = jnp.floor(second * (1.0 / 256.0))
     c = (second - b * 256.0 - 128.0) * 256.0 + (first - a * 256.0)
-    return jnp.concatenate([a * unit, b * unit, c * unit, rest], axis=0).reshape(-1, coded.shape[1])
+    parts = [a * unit, b * unit, c * unit, rest, (level * unit)[None]]
+    return jnp.concatenate([p for p in parts if p.shape[0]], axis=0).reshape(-1, coded.shape[1])
 
 
 def kernel(
@@ -160,9 +148,11 @@
                 self.post(h, 0, 2, -1, 0, 0, 1)
                 self.wait(h, 0, 1, 1, 0)
                 self.post(h, 0, 3, 1, 0, 1, 1)
-            for j in (1, 2):
+            for near_first in (0, 1):
                 for h in (0, 1):
-                    self.second(h, j)
+                    for slot in (0, 1):
+                        j = 1 + (near_first + slot) % 2
+                        self.post(h, 1 + j, slot, OFFSETS[j], 0)
 
         def far_first(self):
             for h in (0, 1):
@@ -170,12 +160,12 @@
                 self.wait(h, 0, 3, 2, 0, 1, 1)
                 self.second(h, 3)
 
-        def relay(self, j):
-            for h in (0, 1):
-                self.wait(h, 1 + j, 0, OFFSETS[j], -1)
-                self.post(h, 1 + j, 2, OFFSETS[j], -1, 0, 1)
-                self.wait(h, 1 + j, 1, OFFSETS[j], 1)
-                self.post(h, 1 + j, 3, OFFSETS[j], 1, 1, 1)
+        def relay(self, minus, plus):
+            for h in (0, 1):
+                for slot, j in ((0, minus), (1, plus)):
+                    by = -1 if slot == 0 else 1
+                    self.wait(h, 1 + j, slot, OFFSETS[j], by)
+                    self.post(h, 1 + j, 2 + slot, OFFSETS[j], by, slot, 1)
 
         def far_second(self, j):
             for h in (0, 1):
@@ -251,7 +241,7 @@
     up.first_axis()
     up_share(1, 0)
     up_share(2, 0)
-    up.relay(0)
+    up.relay(0, 0)
     up_share(0, 1)
     up_share(0, 2)
     up.far_first()
@@ -260,10 +250,10 @@
     tok_post(4, 1, 3, 0, 1)
     tok_wait(3, 2, 1)
     tok_post(5, 2, 3, 1, -1)
-    for j in (1, 2, 3):
-        up.relay(j)
-        up_share(j, 1)
-        up_share(j, 2)
+    for minus, plus in ((1, 2), (2, 1), (3, 3)):
+        up.relay(minus, plus)
+        up_share(minus, 1)
+        up_share(plus, 2)
     dn.start_first()
     dn.start_second()
     tok_wait(1, 1, 1)
@@ -328,23 +318,36 @@
             block = near(z, ORDER[b][0]) * SIDE + near(y, ORDER[b][1])
             pieces.append(dnw[pl.ds(pl.multiple_of(block * 4 * half, 4 * half), 4 * half), :])
         both = dot(hid[...], jnp.concatenate(pieces, axis=1) if len(pieces) > 1 else pieces[0])
-        for i, b in enumerate(group):
-            terms = both[:, i * rows:(i + 1) * rows]
-            for side, by in ((0, 1), (1, -1)):
-                row = 3 * rows + side * (rows // 2)
-                first_out[side, b] = code_pairs(terms[row:row + rows // 2])
-                copy(first_out.at[side, b], first.at[side, b], rs_send, first_recv.at[side, b], device(dx=by)).start()
-            part[b * 3 * rows:(b + 1) * 3 * rows, :] = terms[:3 * rows]
-
-    def pass_on(b):
+        g = GROUPS.index(group)
+        terms = [both[:, i * rows:(i + 1) * rows] for i in range(len(group))]
         for side, by in ((0, 1), (1, -1)):
-            copy(first.at[side, b], first.at[side, b], rs_send, first_recv.at[side, b], device(dx=by)).wait_recv()
+            row = 3 * rows + side * (rows // 2)
+            out, there = first_at(first_out, side, g), first_at(first, side, g)
+            out[...] = code(jnp.concatenate([t[row:row + rows // 2] for t in terms], axis=0))
+            copy(out, there, rs_send, first_recv.at[side, g], device(dx=by)).start()
+        for b, t in zip(group, terms):
+            part[b * 3 * rows:(b + 1) * 3 * rows, :] = t[:3 * rows]
+
+    def first_at(ref, side, g):
+        return ref.at[side, g, 0:coded_rows(len(GROUPS[g]) * rows // 2), :]
+
+    def last_at(ref, side, g):
+        return ref.at[side, g, 0:coded_rows(len(GROUPS[g]) * rows), :]
+
+    def pass_on(g):
+        for side, by in ((0, 1), (1, -1)):
+            here = first_at(first, side, g)
+            copy(here, here, rs_send, first_recv.at[side, g], device(dx=by)).wait_recv()
             slot = 2 - side
-            near_half, far_half = part_at(b, slot, side, 1)[...], part_at(b, slot, 1 - side, 1)[...]
-            summed = near_half + decode_pairs(first[side, b])
-            ordered = [summed, far_half] if side == 0 else [far_half, summed]
-            last_out[side, b] = code_triples(jnp.concatenate(ordered, axis=0))
-            copy(last_out.at[side, b], last.at[side, b], rs_send, last_recv.at[side, b], device(dx=by)).start()
+            got = decode(here[...])
+            ordered = []
+            for i, b in enumerate(GROUPS[g]):
+                summed = part_at(b, slot, side, 1)[...] + got[i * (rows // 2):(i + 1) * (rows // 2)]
+                other = part_at(b, slot, 1 - side, 1)[...]
+                ordered += [summed, other] if side == 0 else [other, summed]
+            out, there = last_at(last_out, side, g), last_at(last, side, g)
+            out[...] = code(jnp.concatenate(ordered, axis=0))
+            copy(out, there, rs_send, last_recv.at[side, g], device(dx=by)).start()
 
     def stored(b):
         block = near(z, ORDER[b][0]) * SIDE + near(y, ORDER[b][1])
@@ -352,50 +355,60 @@
             out_ref.at[b], out_hbm.at[:, pl.ds(pl.multiple_of(block * rows, rows), rows)], store.at[b]
         )
 
-    def finish(b):
+    def finish(g):
         for side, by in ((0, 1), (1, -1)):
-            copy(last.at[side, b], last.at[side, b], rs_send, last_recv.at[side, b], device(dx=by)).wait_recv()
-        total = part_at(b, 0)[...] + decode_triples(last[0, b]) + decode_triples(last[1, b])
-        out_ref[b] = total.astype(BF)
-        stored(b).start()
-
-    def step(g):
-        if g < len(GROUPS):
-            project(GROUPS[g])
-        if 0 <= g - 1 < len(GROUPS):
-            for b in GROUPS[g - 1]:
-                pass_on(b)
-        if 0 <= g - 3 < len(GROUPS):
-            for b in GROUPS[g - 3]:
-                finish(b)
-
-    step(0)
+            here = last_at(last, side, g)
+            copy(here, here, rs_send, last_recv.at[side, g], device(dx=by)).wait_recv()
+        got = decode(last_at(last, 0, g)[...]) + decode(last_at(last, 1, g)[...])
+        for i, b in enumerate(GROUPS[g]):
+            out_ref[b] = (part_at(b, 0)[...] + got[i * rows:(i + 1) * rows]).astype(BF)
+            stored(b).start()
+
+    def share(*bs):
+        for b in bs:
+            dn_share(b)
+
+    project(GROUPS[0])
     dn.first_axis()
-    dn.relay(0)
-    for b in (1, 2, 3, 4):
-        dn_share(b)
+    dn.relay(0, 0)
+    share(1, 2, 3, 4)
+    project(GROUPS[1])
+    pass_on(0)
+    project(GROUPS[2])
     dn.far_first()
-    step(1)
-    dn.relay(1)
-    step(2)
-    dn.relay(2)
-    for b in (5, 6, 7, 8):
-        dn_share(b)
+    pass_on(1)
+    dn.relay(1, 2)
+    share(5, 6)
+    pass_on(2)
+    finish(0)
+    project(GROUPS[3])
+    dn.relay(2, 1)
+    share(7, 8)
     dn.far_second(0)
-    for b in (9, 10):
-        dn_share(b)
-    step(3)
-    dn.relay(3)
-    step(4)
+    share(9, 10)
+    project(GROUPS[4])
+    pass_on(3)
+    project(GROUPS[5])
+    finish(1)
+    dn.relay(3, 3)
+    pass_on(4)
     dn.far_second(1)
+    finish(2)
     dn.far_second(2)
-    for b in (11, 12, 13, 14):
-        dn_share(b)
-    step(5)
+    share(11, 12, 13, 14)
+    pass_on(5)
     dn.far_second(3)
-    dn_share(15)
-    for g in range(6, len(GROUPS) + 3):
-        step(g)
+    share(15)
+    project(GROUPS[6])
+    finish(3)
+    project(GROUPS[7])
+    project(GROUPS[8])
+    pass_on(6)
+    finish(4)
+    pass_on(7)
+    pass_on(8)
+    for g in (5, 6, 7, 8):
+        finish(g)
 
     def drained(ref, sem):
         pltpu.make_async_copy(ref, ref, sem).wait()
@@ -405,7 +418,8 @@
     drained(upw.at[pl.ds(0, 2 * blocks * depth), :], up_pair_send)
     drained(dnw.at[pl.ds(0, blocks * 2 * half), :], dn_pair_send)
     drained(tok.at[pl.ds(0, 3 * rows), :], tok_send)
-    drained(part.at[0:blocks * (5 * rows // 8 + 3 * rows // 2), :], rs_send)
+    sent = sum(coded_rows(len(g) * rows // 2) + coded_rows(len(g) * rows) for g in GROUPS)
+    drained(part.at[0:2 * sent, :], rs_send)
     for b in range(blocks):
         stored(b).wait()
 
@@ -433,11 +447,11 @@
             pltpu.VMEM((SIDE * rows, 2 * inner), F32),
             pltpu.VMEM((SIDE * rows, 2 * inner), BF),
             pltpu.VMEM((blocks * 3 * rows, rows), F32),
-            pltpu.VMEM((2, blocks, 5 * rows // 16, rows), F32),
-            pltpu.VMEM((2, blocks, 3 * rows // 4, rows), F32),
-            pltpu.VMEM((2, blocks, 5 * rows // 16, rows), F32),
-            pltpu.VMEM((2, blocks, 3 * rows // 4, rows), F32),
-            dma((2, 5, 4)), dma((2, 5, 4)), dma((2, 4)), dma((blocks,)), dma((6,)), dma((2, blocks)), dma((2, blocks)),
+            pltpu.VMEM((2, len(GROUPS), coded_rows(rows), rows), F32),
+            pltpu.VMEM((2, len(GROUPS), coded_rows(2 * rows), rows), F32),
+            pltpu.VMEM((2, len(GROUPS), coded_rows(rows), rows), F32),
+            pltpu.VMEM((2, len(GROUPS), coded_rows(2 * rows), rows), F32),
+            dma((2, 5, 4)), dma((2, 5, 4)), dma((2, 4)), dma((blocks,)), dma((6,)), dma((2, len(GROUPS))), dma((2, len(GROUPS))),
             dma, dma, dma, dma, dma, dma, dma((3,)), dma((blocks,)),
         ],
         compiler_params=pltpu.CompilerParams(

time: 74 us -> 72.1 us (0.974)
  Pallas kernels: 71.9 us -> 70 us
    pallas_call x1, Pallas kernels: 71.9 us -> 70 us  [shards(): pl.pallas_call(kernel, out_shape=jax.ShapeDtypeStruct((rows, width), BF),...]
where the time goes in v4:
time: 72.1 us; the launch traced here: 71.9 us
  Pallas kernels  70 us (97%)
  local copies, waits for them, and re-layouts  1.88 us (3%)
    pallas_call x1, Pallas kernels, shards(): pl.pallas_call(kernel, out_shape=jax.ShapeDtypeStruct((rows, width), BF),...  70 us
    unnamed x1, local copies, waits for them, and re-layouts  1.88 us

profile of v4, /device:TPU:1, one launch (start us, length us, event | category | flops | bytes accessed | tf_op | source)
XLA Modules:
  0.0 71.9 jit_solution(2072792028311428677)
XLA Ops:
  0.0 70.0 %shard_map.46 = bf16[128,2048]{1,0:T(8,128)(2,1)} custom-call(bf16[128,2048]{1,0:T(8,128)(2,1)} %tokens_hbm.1, f32[1,2048]{1,0:T(1,128)} %bitcast.1, f32[128,1024]{1,0:T(8,128)} %up_hbm.1, f32[1024,128]{1,0:T(8,128)} %down_hbm.1), custom_call_target="tpu_custom_call" | custom-call | tf_op jit(solution)/shard_map/pallas_call | solution.py:434
  70.0 1.9 %copy.6 = bf16[128,2048]{1,0:T(8,128)(2,1)} copy(bf16[128,2048]{1,0:T(8,128)(2,1)} %shard_map.46) | data formatting | bytes 1048576

commit v5 on v4

--- a/solution.py
+++ b/solution.py
@@ -213,8 +213,13 @@
         row = block * 4 * half + (2 * half if to_partner else 0)
         return dnw.at[pl.ds(pl.multiple_of(row, 2 * half), 2 * half), :]
 
-    def dn_share(b):
-        copy(dn_block(b, False), dn_block(b, True), dn_pair_send, dn_pair.at[b], partner).start()
+    def dn_share(h, *bs):
+        for b in bs:
+            block = near(z, ORDER[b][0]) * SIDE + near(y, ORDER[b][1])
+            mine, theirs = (
+                dnw.at[pl.ds(pl.multiple_of(block * 4 * half + (2 * side + h) * half, half), half), :] for side in (0, 1)
+            )
+            copy(mine, theirs, dn_pair_send, dn_pair.at[b], partner).start()
 
     def up_plane(h, p, to_partner):
         plane = near(z if h == 0 else y, OFFSETS[p])
@@ -236,7 +241,8 @@
             copy(ref, ref, up_pair_send, up_pair.at[h, p], partner).wait_recv()
 
     up_share(0, 0)
-    dn_share(0)
+    for h in (0, 1):
+        dn_share(h, 0)
 
     up.first_axis()
     up_share(1, 0)
@@ -317,7 +323,8 @@
             copy(ref, ref, dn_pair_send, dn_pair.at[b], partner).wait_recv()
             block = near(z, ORDER[b][0]) * SIDE + near(y, ORDER[b][1])
             pieces.append(dnw[pl.ds(pl.multiple_of(block * 4 * half, 4 * half), 4 * half), :])
-        both = dot(hid[...], jnp.concatenate(pieces, axis=1) if len(pieces) > 1 else pieces[0])
+        weights = jnp.concatenate(pieces, axis=1) if len(pieces) > 1 else pieces[0]
+        both = dot(hid[:, :2 * half], weights[:2 * half]) + dot(hid[:, 2 * half:], weights[2 * half:])
         g = GROUPS.index(group)
         terms = [both[:, i * rows:(i + 1) * rows] for i in range(len(group))]
         for side, by in ((0, 1), (1, -1)):
@@ -364,45 +371,55 @@
             out_ref[b] = (part_at(b, 0)[...] + got[i * rows:(i + 1) * rows]).astype(BF)
             stored(b).start()
 
-    def share(*bs):
-        for b in bs:
-            dn_share(b)
-
     project(GROUPS[0])
     dn.first_axis()
+    dn_share(0, 1, 2)
+    dn_share(1, 3, 4)
     dn.relay(0, 0)
-    share(1, 2, 3, 4)
+    dn_share(1, 1, 2)
+    dn_share(0, 3, 4)
     project(GROUPS[1])
     pass_on(0)
     project(GROUPS[2])
     dn.far_first()
+    dn_share(0, 10)
+    dn_share(1, 9)
+    dn.relay(1, 2)
+    for h in (0, 1):
+        dn_share(h, 5, 6)
     pass_on(1)
-    dn.relay(1, 2)
-    share(5, 6)
-    pass_on(2)
     finish(0)
     project(GROUPS[3])
+    pass_on(2)
     dn.relay(2, 1)
-    share(7, 8)
+    for h in (0, 1):
+        dn_share(h, 7, 8)
     dn.far_second(0)
-    share(9, 10)
+    dn_share(0, 9)
+    dn_share(1, 10)
     project(GROUPS[4])
+    project(GROUPS[5])
     pass_on(3)
-    project(GROUPS[5])
+    dn.relay(3, 3)
+    dn_share(0, 11, 13)
+    dn_share(1, 12, 14)
     finish(1)
-    dn.relay(3, 3)
     pass_on(4)
+    finish(2)
     dn.far_second(1)
-    finish(2)
+    dn_share(1, 11)
+    dn_share(0, 12)
     dn.far_second(2)
-    share(11, 12, 13, 14)
+    dn_share(1, 13)
+    dn_share(0, 14)
     pass_on(5)
     dn.far_second(3)
-    share(15)
+    for h in (0, 1):
+        dn_share(h, 15)
     project(GROUPS[6])
-    finish(3)
     project(GROUPS[7])
     project(GROUPS[8])
+    finish(3)
     pass_on(6)
     finish(4)
     pass_on(7)
@@ -455,7 +472,7 @@
             dma, dma, dma, dma, dma, dma, dma((3,)), dma((blocks,)),
         ],
         compiler_params=pltpu.CompilerParams(
-            collective_id=0, has_side_effects=True, vmem_limit_bytes=60 * 1024 * 1024
+            collective_id=0, has_side_effects=True, vmem_limit_bytes=56_000_000
         ),
     )(tokens, norm_gain.reshape(1, width), up_weight, down_weight)
 

time: 72.1 us -> 69.2 us (0.960)
  Pallas kernels: 70 us -> 67.5 us
    pallas_call x1, Pallas kernels: 70 us -> 67.5 us  [shards(): pl.pallas_call(kernel, out_shape=jax.ShapeDtypeStruct((rows, width), BF),...]
    unnamed x1 -> x3, local copies, waits for them, and re-layouts: 1.88 us -> 1.49 us
where the time goes in v5:
time: 69.2 us; the launch traced here: 69 us
  Pallas kernels  67.5 us (98%)
  local copies, waits for them, and re-layouts  1.49 us (2%)
    pallas_call x1, Pallas kernels, shards(): pl.pallas_call(kernel, out_shape=jax.ShapeDtypeStruct((rows, width), BF),...  67.5 us
    unnamed x3, local copies, waits for them, and re-layouts  1.49 us

profile of v5, /device:TPU:1, one launch (start us, length us, event | category | flops | bytes accessed | tf_op | source)
XLA Modules:
  0.0 69.0 jit_solution(6805394280844991487)
XLA Ops:
  0.0 0.0 copy-start
  0.0 0.7 %copy-done = f32[2048]{0:T(1024)S(1)} copy-done((f32[2048]{0:T(1024)S(1)}, f32[2048]{0:T(1024)}, u32[]{:S(2)}) %copy-start) | copy-done | bytes 8216
  0.7 67.5 %shard_map.46 = bf16[128,2048]{1,0:T(8,128)(2,1)S(1)} custom-call(bf16[128,2048]{1,0:T(8,128)(2,1)} %tokens_hbm.1, f32[1,2048]{1,0:T(1,128)S(1)} %bitcast.1, f32[128,1024]{1,0:T(8,128)} %up_hbm.1, f32[1024,128]{1,0:T(8,128)} %down_hbm.1), custom_call_target="tpu_custom_call" | custom-call | tf_op jit(solution)/shard_map/pallas_call | solution.py:451
  68.2 0.8 %copy.6 = bf16[128,2048]{1,0:T(8,128)(2,1)} copy(bf16[128,2048]{1,0:T(8,128)(2,1)S(1)} %shard_map.46) | data formatting | bytes 1048576
Async XLA Ops:
  0.0 0.7 %copy-start = (f32[2048]{0:T(1024)S(1)}, f32[2048]{0:T(1024)}, u32[]{:S(2)}) copy-start(f32[2048]{0:T(1024)} %param.5) | copy-start | bytes 24580

commit v6 on v5

--- a/solution.py
+++ b/solution.py
@@ -58,10 +58,10 @@
 
 
 def kernel(
-    tokens_hbm, gain_ref, up_hbm, down_hbm, out_hbm,
-    tokens_ref, up_ref, down_ref, out_ref, tok, upw, dnw, pre, hid, part, first, last, first_out, last_out,
+    tokens_hbm, gain_ref, up_hbm, down_hbm, out_ref,
+    tokens_ref, up_ref, down_ref, tok, upw, dnw, pre, hid, part, first, last, first_out, last_out,
     up_recv, dn_recv, up_pair, dn_pair, tok_recv, first_recv, last_recv,
-    up_send, dn_send, up_pair_send, dn_pair_send, tok_send, rs_send, load, store,
+    up_send, dn_send, up_pair_send, dn_pair_send, tok_send, rs_send, load,
 ):
     rows, width = tokens_ref.shape
     half = up_ref.shape[1] // 2
@@ -109,71 +109,58 @@
         return dnw.at[pl.ds(pl.multiple_of(row, half // 2), n * (half // 2)), :]
 
     class Gather:
-        def __init__(self, at, recv, send):
-            self.at, self.recv, self.send = at, recv, send
+        def __init__(self, at, span, recv, send):
+            self.at, self.span, self.recv, self.send = at, span, recv, send
 
         def piece(self, h, df, ds, q=0, n=2):
             return self.at(h, ds, df, q, n) if h == 0 else self.at(h, df, ds, q, n)
 
-        def peer(self, h, axis, by):
-            along_y = (h == 0) == (axis == 0)
-            return device(dy=by) if along_y else device(dz=by)
-
-        def post(self, h, stage, slot, df, ds, q=0, n=2):
+        def post(self, h, axis, sem, by, df, ds, q=0, n=2):
             ref = self.piece(h, df, ds, q, n)
-            by = 1 if slot % 2 == 0 else -1
-            copy(ref, ref, self.send, self.recv.at[h, stage, slot], self.peer(h, min(stage, 1), by)).start()
-
-        def wait(self, h, stage, slot, df, ds, q=0, n=2):
-            ref = self.piece(h, df, ds, q, n)
-            copy(ref, ref, self.send, self.recv.at[h, stage, slot], self.peer(h, 0, 1)).wait_recv()
+            to = device(dy=by) if (h == 0) == (axis == 0) else device(dz=by)
+            copy(ref, ref, self.send, self.recv.at[sem], to).start()
+
+        def wait(self, sem, quarters):
+            ref = self.span(quarters)
+            copy(ref, ref, self.send, self.recv.at[sem], partner).wait_recv()
 
         def start_first(self):
             for h in (0, 1):
-                for slot in (0, 1):
-                    self.post(h, 0, slot, 0, 0)
+                for by in (1, -1):
+                    self.post(h, 0, 0, by, 0, 0)
 
         def start_second(self):
             for h in (0, 1):
-                for slot in (0, 1):
-                    self.post(h, 1, slot, 0, 0)
-
-        def second(self, h, j):
-            for slot in (0, 1):
-                self.post(h, 1 + j, slot, OFFSETS[j], 0)
+                for by in (1, -1):
+                    self.post(h, 1, 2, by, 0, 0)
 
         def first_axis(self):
+            self.wait(0, 8)
             for h in (0, 1):
-                self.wait(h, 0, 0, -1, 0)
-                self.post(h, 0, 2, -1, 0, 0, 1)
-                self.wait(h, 0, 1, 1, 0)
-                self.post(h, 0, 3, 1, 0, 1, 1)
-            for near_first in (0, 1):
+                for q, by in ((0, 1), (1, -1)):
+                    self.post(h, 0, 1, by, -by, 0, q, 1)
+            for turn in (0, 1):
                 for h in (0, 1):
-                    for slot in (0, 1):
-                        j = 1 + (near_first + slot) % 2
-                        self.post(h, 1 + j, slot, OFFSETS[j], 0)
+                    for by in (1, -1):
+                        self.post(h, 1, 3 + turn, by, -by if turn == 0 else by, 0)
 
         def far_first(self):
+            self.wait(1, 4)
             for h in (0, 1):
-                self.wait(h, 0, 2, 2, 0, 0, 1)
-                self.wait(h, 0, 3, 2, 0, 1, 1)
-                self.second(h, 3)
+                for by in (1, -1):
+                    self.post(h, 1, 5, by, 2, 0)
 
         def relay(self, minus, plus):
+            self.wait(2 + minus, 8)
             for h in (0, 1):
-                for slot, j in ((0, minus), (1, plus)):
-                    by = -1 if slot == 0 else 1
-                    self.wait(h, 1 + j, slot, OFFSETS[j], by)
-                    self.post(h, 1 + j, 2 + slot, OFFSETS[j], by, slot, 1)
+                for q, by, j in ((0, 1, minus), (1, -1, plus)):
+                    self.post(h, 1, 6 + j, by, OFFSETS[j], -by, q, 1)
 
         def far_second(self, j):
-            for h in (0, 1):
-                self.wait(h, 1 + j, 2, OFFSETS[j], 2, 0, 1)
-                self.wait(h, 1 + j, 3, OFFSETS[j], 2, 1, 1)
-
-    up = Gather(up_at, up_recv, up_send)
-    dn = Gather(dn_at, dn_recv, dn_send)
+            self.wait(6 + j, 4)
+
+    up = Gather(up_at, lambda n: upw.at[0:n * (depth // 2), :], up_recv, up_send)
+    dn = Gather(dn_at, lambda n: dnw.at[0:n * (half // 2), :], dn_recv, dn_send)
 
     loads[0].wait()
     for h in (0, 1):
@@ -195,13 +182,14 @@
     def tok_post(sem, slot, there, q, by):
         copy(tok_at(slot, q), tok_at(there, q), tok_send, tok_recv.at[sem], device(dx=by)).start()
 
-    def tok_wait(sem, slot, q):
-        copy(tok_at(slot, q), tok_at(slot, q), tok_send, tok_recv.at[sem], device(dx=1)).wait_recv()
+    def tok_wait(sem, halves):
+        ref = tok.at[0:halves * (rows // 2), :]
+        copy(ref, ref, tok_send, tok_recv.at[sem], partner).wait_recv()
 
     tok_post(0, 0, 1, 0, 1)
-    tok_post(3, 0, 2, 1, -1)
+    tok_post(0, 0, 2, 1, -1)
     tok_post(1, 0, 1, 1, 1)
-    tok_post(2, 0, 2, 0, -1)
+    tok_post(1, 0, 2, 0, -1)
     up.start_second()
     loads[2].wait()
 
@@ -219,7 +207,7 @@
             mine, theirs = (
                 dnw.at[pl.ds(pl.multiple_of(block * 4 * half + (2 * side + h) * half, half), half), :] for side in (0, 1)
             )
-            copy(mine, theirs, dn_pair_send, dn_pair.at[b], partner).start()
+            copy(mine, theirs, dn_pair_send, dn_pair.at[(b + 1) // 2], partner).start()
 
     def up_plane(h, p, to_partner):
         plane = near(z if h == 0 else y, OFFSETS[p])
@@ -233,12 +221,11 @@
             mine, theirs = (
                 upw.at[pl.ds(pl.multiple_of((h + 2 * side) * blocks * depth + row, depth), depth), :] for side in (0, 1)
             )
-            copy(mine, theirs, up_pair_send, up_pair.at[h, p], partner).start()
+            copy(mine, theirs, up_pair_send, up_pair.at[p], partner).start()
 
     def up_shared(p):
-        for h in (0, 1):
-            ref = up_plane(h, p, True)
-            copy(ref, ref, up_pair_send, up_pair.at[h, p], partner).wait_recv()
+        ref = upw.at[0:2 * SIDE * depth, :]
+        copy(ref, ref, up_pair_send, up_pair.at[p], partner).wait_recv()
 
     up_share(0, 0)
     for h in (0, 1):
@@ -252,20 +239,16 @@
     up_share(0, 2)
     up.far_first()
     up_share(3, 0)
-    tok_wait(0, 1, 0)
-    tok_post(4, 1, 3, 0, 1)
-    tok_wait(3, 2, 1)
-    tok_post(5, 2, 3, 1, -1)
+    tok_wait(0, 2)
+    tok_post(1, 1, 3, 0, 1)
+    tok_post(1, 2, 3, 1, -1)
     for minus, plus in ((1, 2), (2, 1), (3, 3)):
         up.relay(minus, plus)
         up_share(minus, 1)
         up_share(plus, 2)
     dn.start_first()
     dn.start_second()
-    tok_wait(1, 1, 1)
-    tok_wait(2, 2, 0)
-    tok_wait(4, 3, 0)
-    tok_wait(5, 3, 1)
+    tok_wait(1, 4)
 
     def columns_of(h, p):
         plane = near(z if h == 0 else y, OFFSETS[p])
@@ -318,20 +301,20 @@
 
     def project(group):
         pieces = []
+        g = GROUPS.index(group)
+        ref = dnw.at[0:len(group) * 2 * half, :]
+        copy(ref, ref, dn_pair_send, dn_pair.at[g], partner).wait_recv()
         for b in group:
-            ref = dn_block(b, True)
-            copy(ref, ref, dn_pair_send, dn_pair.at[b], partner).wait_recv()
             block = near(z, ORDER[b][0]) * SIDE + near(y, ORDER[b][1])
             pieces.append(dnw[pl.ds(pl.multiple_of(block * 4 * half, 4 * half), 4 * half), :])
         weights = jnp.concatenate(pieces, axis=1) if len(pieces) > 1 else pieces[0]
-        both = dot(hid[:, :2 * half], weights[:2 * half]) + dot(hid[:, 2 * half:], weights[2 * half:])
-        g = GROUPS.index(group)
+        both = jnp.concatenate([dot(hid[at:at + 2 * rows, :], weights) for at in (0, 2 * rows)], axis=0)
         terms = [both[:, i * rows:(i + 1) * rows] for i in range(len(group))]
         for side, by in ((0, 1), (1, -1)):
             row = 3 * rows + side * (rows // 2)
             out, there = first_at(first_out, side, g), first_at(first, side, g)
             out[...] = code(jnp.concatenate([t[row:row + rows // 2] for t in terms], axis=0))
-            copy(out, there, rs_send, first_recv.at[side, g], device(dx=by)).start()
+            copy(out, there, rs_send, first_recv.at[g], device(dx=by)).start()
         for b, t in zip(group, terms):
             part[b * 3 * rows:(b + 1) * 3 * rows, :] = t[:3 * rows]
 
@@ -342,11 +325,11 @@
         return ref.at[side, g, 0:coded_rows(len(GROUPS[g]) * rows), :]
 
     def pass_on(g):
+        came = part.at[0:2 * coded_rows(len(GROUPS[g]) * rows // 2), :]
+        copy(came, came, rs_send, first_recv.at[g], partner).wait_recv()
         for side, by in ((0, 1), (1, -1)):
-            here = first_at(first, side, g)
-            copy(here, here, rs_send, first_recv.at[side, g], device(dx=by)).wait_recv()
             slot = 2 - side
-            got = decode(here[...])
+            got = decode(first_at(first, side, g)[...])
             ordered = []
             for i, b in enumerate(GROUPS[g]):
                 summed = part_at(b, slot, side, 1)[...] + got[i * (rows // 2):(i + 1) * (rows // 2)]
@@ -354,27 +337,21 @@
                 ordered += [summed, other] if side == 0 else [other, summed]
             out, there = last_at(last_out, side, g), last_at(last, side, g)
             out[...] = code(jnp.concatenate(ordered, axis=0))
-            copy(out, there, rs_send, last_recv.at[side, g], device(dx=by)).start()
-
-    def stored(b):
-        block = near(z, ORDER[b][0]) * SIDE + near(y, ORDER[b][1])
-        return pltpu.make_async_copy(
-            out_ref.at[b], out_hbm.at[:, pl.ds(pl.multiple_of(block * rows, rows), rows)], store.at[b]
-        )
+            copy(out, there, rs_send, last_recv.at[g], device(dx=by)).start()
 
     def finish(g):
-        for side, by in ((0, 1), (1, -1)):
-            here = last_at(last, side, g)
-            copy(here, here, rs_send, last_recv.at[side, g], device(dx=by)).wait_recv()
+        came = part.at[0:2 * coded_rows(len(GROUPS[g]) * rows), :]
+        copy(came, came, rs_send, last_recv.at[g], partner).wait_recv()
         got = decode(last_at(last, 0, g)[...]) + decode(last_at(last, 1, g)[...])
         for i, b in enumerate(GROUPS[g]):
-            out_ref[b] = (part_at(b, 0)[...] + got[i * rows:(i + 1) * rows]).astype(BF)
-            stored(b).start()
-
-    project(GROUPS[0])
+            block = near(z, ORDER[b][0]) * SIDE + near(y, ORDER[b][1])
+            total = part_at(b, 0)[...] + got[i * rows:(i + 1) * rows]
+            out_ref[:, pl.ds(pl.multiple_of(block * rows, rows), rows)] = total.astype(BF)
+
     dn.first_axis()
     dn_share(0, 1, 2)
     dn_share(1, 3, 4)
+    project(GROUPS[0])
     dn.relay(0, 0)
     dn_share(1, 1, 2)
     dn_share(0, 3, 4)
@@ -412,12 +389,12 @@
     dn.far_second(2)
     dn_share(1, 13)
     dn_share(0, 14)
+    project(GROUPS[6])
+    dn.far_second(3)
+    for h in (0, 1):
+        dn_share(h, 15)
+    project(GROUPS[7])
     pass_on(5)
-    dn.far_second(3)
-    for h in (0, 1):
-        dn_share(h, 15)
-    project(GROUPS[6])
-    project(GROUPS[7])
     project(GROUPS[8])
     finish(3)
     pass_on(6)
@@ -437,8 +414,6 @@
     drained(tok.at[pl.ds(0, 3 * rows), :], tok_send)
     sent = sum(coded_rows(len(g) * rows // 2) + coded_rows(len(g) * rows) for g in GROUPS)
     drained(part.at[0:2 * sent, :], rs_send)
-    for b in range(blocks):
-        stored(b).wait()
 
 
 def shards(tokens, norm_gain, up_weight, down_weight):
@@ -452,12 +427,11 @@
         kernel,
         out_shape=jax.ShapeDtypeStruct((rows, width), BF),
         in_specs=[anywhere, vmem, anywhere, anywhere],
-        out_specs=anywhere,
+        out_specs=vmem,
         scratch_shapes=[
             pltpu.VMEM(tokens.shape, BF),
             pltpu.VMEM(up_weight.shape, F32),
             pltpu.VMEM(down_weight.shape, F32),
-            pltpu.VMEM((blocks, rows, rows), BF),
             pltpu.VMEM((SIDE * rows, width), BF),
             pltpu.VMEM((4 * blocks * depth, inner // 2), BF),
             pltpu.VMEM((blocks * 2 * inner, rows), BF),
@@ -468,8 +442,8 @@
             pltpu.VMEM((2, len(GROUPS), coded_rows(2 * rows), rows), F32),
             pltpu.VMEM((2, len(GROUPS), coded_rows(rows), rows), F32),
             pltpu.VMEM((2, len(GROUPS), coded_rows(2 * rows), rows), F32),
-            dma((2, 5, 4)), dma((2, 5, 4)), dma((2, 4)), dma((blocks,)), dma((6,)), dma((2, len(GROUPS))), dma((2, len(GROUPS))),
-            dma, dma, dma, dma, dma, dma, dma((3,)), dma((blocks,)),
+            dma((10,)), dma((10,)), dma((4,)), dma((len(GROUPS),)), dma((2,)), dma((len(GROUPS),)), dma((len(GROUPS),)),
+            dma, dma, dma, dma, dma, dma, dma((3,)),
         ],
         compiler_params=pltpu.CompilerParams(
             collective_id=0, has_side_effects=True, vmem_limit_bytes=56_000_000

time: 69.2 us -> 67.1 us (0.970)
  Pallas kernels: 67.5 us -> 65.5 us
    pallas_call x1, Pallas kernels: 67.5 us -> 65.5 us  [shards(): pl.pallas_call(kernel, out_shape=jax.ShapeDtypeStruct((rows, width), BF),...]
where the time goes in v6:
time: 67.1 us; the launch traced here: 67 us
  Pallas kernels  65.5 us (98%)
  local copies, waits for them, and re-layouts  1.49 us (2%)
    pallas_call x1, Pallas kernels, shards(): pl.pallas_call(kernel, out_shape=jax.ShapeDtypeStruct((rows, width), BF),...  65.5 us
    unnamed x3, local copies, waits for them, and re-layouts  1.49 us

profile of v6, /device:TPU:1, one launch (start us, length us, event | category | flops | bytes accessed | tf_op | source)
XLA Modules:
  0.0 67.0 jit_solution(17421087647772218168)
XLA Ops:
  0.0 0.0 copy-start
  0.0 0.7 %copy-done = f32[2048]{0:T(1024)S(1)} copy-done((f32[2048]{0:T(1024)S(1)}, f32[2048]{0:T(1024)}, u32[]{:S(2)}) %copy-start) | copy-done | bytes 8216
  0.7 65.5 %shard_map.46 = bf16[128,2048]{1,0:T(8,128)(2,1)S(1)} custom-call(bf16[128,2048]{1,0:T(8,128)(2,1)} %tokens_hbm.1, f32[1,2048]{1,0:T(1,128)S(1)} %bitcast.1, f32[128,1024]{1,0:T(8,128)} %up_hbm.1, f32[1024,128]{1,0:T(8,128)} %down_hbm.1), custom_call_target="tpu_custom_call" | custom-call | tf_op jit(solution)/shard_map/pallas_call | solution.py:426
  66.2 0.8 %copy.6 = bf16[128,2048]{1,0:T(8,128)(2,1)} copy(bf16[128,2048]{1,0:T(8,128)(2,1)S(1)} %shard_map.46) | data formatting | bytes 1048576
Async XLA Ops:
  0.0 0.7 %copy-start = (f32[2048]{0:T(1024)S(1)}, f32[2048]{0:T(1024)}, u32[]{:S(2)}) copy-start(f32[2048]{0:T(1024)} %param.5) | copy-start | bytes 24580

commit v7 on v6

--- a/solution.py
+++ b/solution.py
@@ -25,36 +25,34 @@
 GROUPS = ((0,), (1, 2), (3, 4), (5, 6), (7, 8), (9, 10), (11, 12), (13, 14), (15,))
 
 
+LEVELS = 248 * 128 - 1
+LOWEST = 123.0
+
+
 def coded_rows(rows):
-    n = rows // 8
-    return 8 * (2 * (n // 3) + n % 3)
+    return rows + 16
 
 
 def code(values):
     groups = values.reshape(-1, 8, values.shape[1])
     top = jnp.maximum(jnp.max(jnp.abs(groups), axis=0), 1e-20)
-    exponent = jnp.ceil(jnp.log2(top * (1.0 / 32767.0)) + 0.001)
-    inverse = jnp.exp2(-exponent)
-    n = groups.shape[0] // 3
-    a, b, c = (jnp.round(groups[i * n:(i + 1) * n] * inverse) for i in range(3))
-    last = jnp.round(groups[-1] * inverse) * 256.0 + (exponent + 128.0)
-    high = jnp.floor(c * (1.0 / 256.0))
-    low = c - high * 256.0
-    parts = [a * 256.0 + low, b * 256.0 + (high + 128.0), groups[3 * n:-1], last[None]]
-    return jnp.concatenate([p for p in parts if p.shape[0]], axis=0).reshape(-1, values.shape[1])
+    exponent = jnp.ceil(jnp.log2(top * (1.0 / LEVELS)) + 0.001)
+    scaled = groups * jnp.exp2(-exponent)
+    level = jnp.round(jnp.abs(scaled))
+    e = jnp.floor(level * (1.0 / 128.0))
+    word = jnp.exp2(e - LOWEST) * (level * (1.0 / 128.0) + (1.0 - e))
+    word = jnp.where(scaled < 0.0, -word, word)
+    both = jnp.concatenate([word, exponent[None], exponent[None]], axis=0)
+    return both.reshape(-1, values.shape[1]).astype(BF)
 
 
 def decode(coded):
-    groups = coded.reshape(-1, 8, coded.shape[1])
-    n = groups.shape[0] // 2 if groups.shape[0] % 2 else groups.shape[0] // 2 - 1
-    first, second, rest = groups[:n], groups[n:2 * n], groups[2 * n:-1]
-    level = jnp.floor(groups[-1] * (1.0 / 256.0))
-    unit = jnp.exp2(groups[-1] - level * 256.0 - 128.0)
-    a = jnp.floor(first * (1.0 / 256.0))
-    b = jnp.floor(second * (1.0 / 256.0))
-    c = (second - b * 256.0 - 128.0) * 256.0 + (first - a * 256.0)
-    parts = [a * unit, b * unit, c * unit, rest, (level * unit)[None]]
-    return jnp.concatenate([p for p in parts if p.shape[0]], axis=0).reshape(-1, coded.shape[1])
+    groups = coded.astype(F32).reshape(-1, 8, coded.shape[1])
+    words, unit = groups[:-2], jnp.exp2(groups[-1])
+    size = jnp.abs(words)
+    e = jnp.floor(jnp.log2(size) + 0.001)
+    level = (e + size * jnp.exp2(-e)) * 128.0 + (LOWEST - 1.0) * 128.0
+    return (jnp.where(words < 0.0, -level, level) * unit).reshape(-1, coded.shape[1])
 
 
 def kernel(
@@ -227,6 +225,7 @@
         ref = upw.at[0:2 * SIDE * depth, :]
         copy(ref, ref, up_pair_send, up_pair.at[p], partner).wait_recv()
 
+    dn.start_first()
     up_share(0, 0)
     for h in (0, 1):
         dn_share(h, 0)
@@ -246,8 +245,10 @@
         up.relay(minus, plus)
         up_share(minus, 1)
         up_share(plus, 2)
-    dn.start_first()
     dn.start_second()
+    dn.first_axis()
+    dn_share(0, 1, 2)
+    dn_share(1, 3, 4)
     tok_wait(1, 4)
 
     def columns_of(h, p):
@@ -325,7 +326,7 @@
         return ref.at[side, g, 0:coded_rows(len(GROUPS[g]) * rows), :]
 
     def pass_on(g):
-        came = part.at[0:2 * coded_rows(len(GROUPS[g]) * rows // 2), :]
+        came = dnw.at[0:2 * coded_rows(len(GROUPS[g]) * rows // 2), :]
         copy(came, came, rs_send, first_recv.at[g], partner).wait_recv()
         for side, by in ((0, 1), (1, -1)):
             slot = 2 - side
@@ -340,7 +341,7 @@
             copy(out, there, rs_send, last_recv.at[g], device(dx=by)).start()
 
     def finish(g):
-        came = part.at[0:2 * coded_rows(len(GROUPS[g]) * rows), :]
+        came = dnw.at[0:2 * coded_rows(len(GROUPS[g]) * rows), :]
         copy(came, came, rs_send, last_recv.at[g], partner).wait_recv()
         got = decode(last_at(last, 0, g)[...]) + decode(last_at(last, 1, g)[...])
         for i, b in enumerate(GROUPS[g]):
@@ -348,24 +349,20 @@
             total = part_at(b, 0)[...] + got[i * rows:(i + 1) * rows]
             out_ref[:, pl.ds(pl.multiple_of(block * rows, rows), rows)] = total.astype(BF)
 
-    dn.first_axis()
-    dn_share(0, 1, 2)
-    dn_share(1, 3, 4)
     project(GROUPS[0])
     dn.relay(0, 0)
     dn_share(1, 1, 2)
     dn_share(0, 3, 4)
-    project(GROUPS[1])
-    pass_on(0)
-    project(GROUPS[2])
     dn.far_first()
     dn_share(0, 10)
     dn_share(1, 9)
+    project(GROUPS[1])
+    project(GROUPS[2])
+    pass_on(0)
     dn.relay(1, 2)
     for h in (0, 1):
         dn_share(h, 5, 6)
     pass_on(1)
-    finish(0)
     project(GROUPS[3])
     pass_on(2)
     dn.relay(2, 1)
@@ -374,6 +371,7 @@
     dn.far_second(0)
     dn_share(0, 9)
     dn_share(1, 10)
+    finish(0)
     project(GROUPS[4])
     project(GROUPS[5])
     pass_on(3)
@@ -381,11 +379,10 @@
     dn_share(0, 11, 13)
     dn_share(1, 12, 14)
     finish(1)
-    pass_on(4)
-    finish(2)
     dn.far_second(1)
     dn_share(1, 11)
     dn_share(0, 12)
+    pass_on(4)
     dn.far_second(2)
     dn_share(1, 13)
     dn_share(0, 14)
@@ -396,6 +393,7 @@
     project(GROUPS[7])
     pass_on(5)
     project(GROUPS[8])
+    finish(2)
     finish(3)
     pass_on(6)
     finish(4)
@@ -413,7 +411,7 @@
     drained(dnw.at[pl.ds(0, blocks * 2 * half), :], dn_pair_send)
     drained(tok.at[pl.ds(0, 3 * rows), :], tok_send)
     sent = sum(coded_rows(len(g) * rows // 2) + coded_rows(len(g) * rows) for g in GROUPS)
-    drained(part.at[0:2 * sent, :], rs_send)
+    drained(dnw.at[0:2 * sent, :], rs_send)
 
 
 def shards(tokens, norm_gain, up_weight, down_weight):
@@ -438,10 +436,10 @@
             pltpu.VMEM((SIDE * rows, 2 * inner), F32),
             pltpu.VMEM((SIDE * rows, 2 * inner), BF),
             pltpu.VMEM((blocks * 3 * rows, rows), F32),
-            pltpu.VMEM((2, len(GROUPS), coded_rows(rows), rows), F32),
-            pltpu.VMEM((2, len(GROUPS), coded_rows(2 * rows), rows), F32),
-            pltpu.VMEM((2, len(GROUPS), coded_rows(rows), rows), F32),
-            pltpu.VMEM((2, len(GROUPS), coded_rows(2 * rows), rows), F32),
+            pltpu.VMEM((2, len(GROUPS), coded_rows(rows), rows), BF),
+            pltpu.VMEM((2, len(GROUPS), coded_rows(2 * rows), rows), BF),
+            pltpu.VMEM((2, len(GROUPS), coded_rows(rows), rows), BF),
+            pltpu.VMEM((2, len(GROUPS), coded_rows(2 * rows), rows), BF),
             dma((10,)), dma((10,)), dma((4,)), dma((len(GROUPS),)), dma((2,)), dma((len(GROUPS),)), dma((len(GROUPS),)),
             dma, dma, dma, dma, dma, dma, dma((3,)),
         ],

time: 67.1 us -> 64.6 us (0.963)
  Pallas kernels: 65.5 us -> 62.9 us
    pallas_call x1, Pallas kernels: 65.5 us -> 62.9 us  [shards(): pl.pallas_call(kernel, out_shape=jax.ShapeDtypeStruct((rows, width), BF),...]
where the time goes in v7:
time: 64.6 us; the launch traced here: 64.4 us
  Pallas kernels  62.9 us (97%)
  local copies, waits for them, and re-layouts  1.49 us (2%)
    pallas_call x1, Pallas kernels, shards(): pl.pallas_call(kernel, out_shape=jax.ShapeDtypeStruct((rows, width), BF),...  62.9 us
    unnamed x3, local copies, waits for them, and re-layouts  1.49 us

profile of v7, /device:TPU:1, one launch (start us, length us, event | category | flops | bytes accessed | tf_op | source)
XLA Modules:
  0.0 64.4 jit_solution(14256078844414714616)
XLA Ops:
  0.0 0.0 copy-start
  0.0 0.7 %copy-done = f32[2048]{0:T(1024)S(1)} copy-done((f32[2048]{0:T(1024)S(1)}, f32[2048]{0:T(1024)}, u32[]{:S(2)}) %copy-start) | copy-done | bytes 8216
  0.7 62.9 %shard_map.46 = bf16[128,2048]{1,0:T(8,128)(2,1)S(1)} custom-call(bf16[128,2048]{1,0:T(8,128)(2,1)} %tokens_hbm.1, f32[1,2048]{1,0:T(1,128)S(1)} %bitcast.1, f32[128,1024]{1,0:T(8,128)} %up_hbm.1, f32[1024,128]{1,0:T(8,128)} %down_hbm.1), custom_call_target="tpu_custom_call" | custom-call | tf_op jit(solution)/shard_map/pallas_call | solution.py:424
  63.6 0.8 %copy.6 = bf16[128,2048]{1,0:T(8,128)(2,1)} copy(bf16[128,2048]{1,0:T(8,128)(2,1)S(1)} %shard_map.46) | data formatting | bytes 1048576
Async XLA Ops:
  0.0 0.7 %copy-start = (f32[2048]{0:T(1024)S(1)}, f32[2048]{0:T(1024)}, u32[]{:S(2)}) copy-start(f32[2048]{0:T(1024)} %param.5) | copy-start | bytes 24580

commit v8 on v7

--- a/solution.py
+++ b/solution.py
@@ -92,8 +92,7 @@
         pltpu.make_async_copy(src, dst, load.at[i])
         for i, (src, dst) in enumerate(((up_hbm, up_ref), (tokens_hbm, tokens_ref), (down_hbm, down_ref)))
     ]
-    for one in loads:
-        one.start()
+    loads[0].start()
 
     def up_at(h, dz, dy, q, n):
         zs, ys = near(z, dz), near(y, dy)
@@ -161,6 +160,8 @@
     dn = Gather(dn_at, lambda n: dnw.at[0:n * (half // 2), :], dn_recv, dn_send)
 
     loads[0].wait()
+    loads[1].start()
+    loads[2].start()
     for h in (0, 1):
         block = fs if h == 0 else y * SIDE + z
         row = pl.multiple_of(h * blocks * depth + block * depth, depth)
@@ -353,10 +354,10 @@
     dn.relay(0, 0)
     dn_share(1, 1, 2)
     dn_share(0, 3, 4)
+    project(GROUPS[1])
     dn.far_first()
     dn_share(0, 10)
     dn_share(1, 9)
-    project(GROUPS[1])
     project(GROUPS[2])
     pass_on(0)
     dn.relay(1, 2)
@@ -364,20 +365,20 @@
         dn_share(h, 5, 6)
     pass_on(1)
     project(GROUPS[3])
+    dn.relay(2, 1)
+    for h in (0, 1):
+        dn_share(h, 7, 8)
     pass_on(2)
-    dn.relay(2, 1)
-    for h in (0, 1):
-        dn_share(h, 7, 8)
     dn.far_second(0)
     dn_share(0, 9)
     dn_share(1, 10)
+    project(GROUPS[4])
     finish(0)
-    project(GROUPS[4])
     project(GROUPS[5])
-    pass_on(3)
     dn.relay(3, 3)
     dn_share(0, 11, 13)
     dn_share(1, 12, 14)
+    pass_on(3)
     finish(1)
     dn.far_second(1)
     dn_share(1, 11)
@@ -387,14 +388,14 @@
     dn_share(1, 13)
     dn_share(0, 14)
     project(GROUPS[6])
-    dn.far_second(3)
-    for h in (0, 1):
-        dn_share(h, 15)
     project(GROUPS[7])
     pass_on(5)
-    project(GROUPS[8])
+    dn.far_second(3)
+    for h in (0, 1):
+        dn_share(h, 15)
     finish(2)
     finish(3)
+    project(GROUPS[8])
     pass_on(6)
     finish(4)
     pass_on(7)

time: 64.6 us -> 63.8 us (0.988)
  Pallas kernels: 62.9 us -> 62.1 us
    pallas_call x1, Pallas kernels: 62.9 us -> 62.1 us  [shards(): pl.pallas_call(kernel, out_shape=jax.ShapeDtypeStruct((rows, width), BF),...]
where the time goes in v8:
time: 63.8 us; the launch traced here: 63.6 us
  Pallas kernels  62.1 us (97%)
  local copies, waits for them, and re-layouts  1.49 us (2%)
    pallas_call x1, Pallas kernels, shards(): pl.pallas_call(kernel, out_shape=jax.ShapeDtypeStruct((rows, width), BF),...  62.1 us
    unnamed x3, local copies, waits for them, and re-layouts  1.49 us

profile of v8, /device:TPU:1, one launch (start us, length us, event | category | flops | bytes accessed | tf_op | source)
XLA Modules:
  0.0 63.6 jit_solution(12687004701851154137)
XLA Ops:
  0.0 0.0 copy-start
  0.0 0.7 %copy-done = f32[2048]{0:T(1024)S(1)} copy-done((f32[2048]{0:T(1024)S(1)}, f32[2048]{0:T(1024)}, u32[]{:S(2)}) %copy-start) | copy-done | bytes 8216
  0.7 62.1 %shard_map.46 = bf16[128,2048]{1,0:T(8,128)(2,1)S(1)} custom-call(bf16[128,2048]{1,0:T(8,128)(2,1)} %tokens_hbm.1, f32[1,2048]{1,0:T(1,128)S(1)} %bitcast.1, f32[128,1024]{1,0:T(8,128)} %up_hbm.1, f32[1024,128]{1,0:T(8,128)} %down_hbm.1), custom_call_target="tpu_custom_call" | custom-call | tf_op jit(solution)/shard_map/pallas_call | solution.py:425
  62.8 0.8 %copy.6 = bf16[128,2048]{1,0:T(8,128)(2,1)} copy(bf16[128,2048]{1,0:T(8,128)(2,1)S(1)} %shard_map.46) | data formatting | bytes 1048576
Async XLA Ops:
  0.0 0.7 %copy-start = (f32[2048]{0:T(1024)S(1)}, f32[2048]{0:T(1024)}, u32[]{:S(2)}) copy-start(f32[2048]{0:T(1024)} %param.5) | copy-start | bytes 24580

commit v9 on v8

--- a/solution.py
+++ b/solution.py
@@ -293,6 +293,17 @@
         up_share(j, 3)
     for h in (0, 1):
         late(h, 0)
+    def near_own():
+        dn.relay(0, 0)
+        dn_share(1, 1, 2)
+        dn_share(0, 3, 4)
+
+    def farthest():
+        dn.far_second(3)
+        for h in (0, 1):
+            dn_share(h, 15)
+
+    pl.when(core == 1)(near_own)
     up_shared(3)
     for h in (0, 1):
         late(h, 1)
@@ -302,15 +313,24 @@
         return part.at[row:row + n * (rows // 2), :]
 
     def project(group):
-        pieces = []
         g = GROUPS.index(group)
+
+        def product(depth_from, depth_to):
+            pieces = []
+            for b in group:
+                block = near(z, ORDER[b][0]) * SIDE + near(y, ORDER[b][1])
+                row = pl.multiple_of(block * 4 * half + depth_from, half)
+                pieces.append(dnw[pl.ds(row, depth_to - depth_from), :])
+            weights = jnp.concatenate(pieces, axis=1) if len(pieces) > 1 else pieces[0]
+            parts = [dot(hid[at:at + 2 * rows, depth_from:depth_to], weights) for at in (0, 2 * rows)]
+            return jnp.concatenate(parts, axis=0)
+
+        last_group = g == len(GROUPS) - 1
+        if last_group:
+            pre[:, :rows] = product(0, 2 * half)
         ref = dnw.at[0:len(group) * 2 * half, :]
         copy(ref, ref, dn_pair_send, dn_pair.at[g], partner).wait_recv()
-        for b in group:
-            block = near(z, ORDER[b][0]) * SIDE + near(y, ORDER[b][1])
-            pieces.append(dnw[pl.ds(pl.multiple_of(block * 4 * half, 4 * half), 4 * half), :])
-        weights = jnp.concatenate(pieces, axis=1) if len(pieces) > 1 else pieces[0]
-        both = jnp.concatenate([dot(hid[at:at + 2 * rows, :], weights) for at in (0, 2 * rows)], axis=0)
+        both = pre[:, :rows] + product(2 * half, 4 * half) if last_group else product(0, 4 * half)
         terms = [both[:, i * rows:(i + 1) * rows] for i in range(len(group))]
         for side, by in ((0, 1), (1, -1)):
             row = 3 * rows + side * (rows // 2)
@@ -351,9 +371,7 @@
             out_ref[:, pl.ds(pl.multiple_of(block * rows, rows), rows)] = total.astype(BF)
 
     project(GROUPS[0])
-    dn.relay(0, 0)
-    dn_share(1, 1, 2)
-    dn_share(0, 3, 4)
+    pl.when(core == 0)(near_own)
     project(GROUPS[1])
     dn.far_first()
     dn_share(0, 10)
@@ -388,11 +406,10 @@
     dn_share(1, 13)
     dn_share(0, 14)
     project(GROUPS[6])
+    pl.when(core == 1)(farthest)
     project(GROUPS[7])
     pass_on(5)
-    dn.far_second(3)
-    for h in (0, 1):
-        dn_share(h, 15)
+    pl.when(core == 0)(farthest)
     finish(2)
     finish(3)
     project(GROUPS[8])

time: 63.8 us -> 63.6 us (level)
  no operation moved by 1% of the time
where the time goes in v9:
time: 63.6 us; the launch traced here: 63.4 us
  Pallas kernels  61.9 us (97%)
  local copies, waits for them, and re-layouts  1.49 us (2%)
    pallas_call x1, Pallas kernels, shards(): pl.pallas_call(kernel, out_shape=jax.ShapeDtypeStruct((rows, width), BF),...  61.9 us
    unnamed x3, local copies, waits for them, and re-layouts  1.49 us

profile of v9, /device:TPU:1, one launch (start us, length us, event | category | flops | bytes accessed | tf_op | source)
XLA Modules:
  0.0 63.4 jit_solution(11165804582053801934)
XLA Ops:
  0.0 0.0 copy-start
  0.0 0.7 %copy-done = f32[2048]{0:T(1024)S(1)} copy-done((f32[2048]{0:T(1024)S(1)}, f32[2048]{0:T(1024)}, u32[]{:S(2)}) %copy-start) | copy-done | bytes 8216
  0.7 61.9 %shard_map.46 = bf16[128,2048]{1,0:T(8,128)(2,1)S(1)} custom-call(bf16[128,2048]{1,0:T(8,128)(2,1)} %tokens_hbm.1, f32[1,2048]{1,0:T(1,128)S(1)} %bitcast.1, f32[128,1024]{1,0:T(8,128)} %up_hbm.1, f32[1024,128]{1,0:T(8,128)} %down_hbm.1), custom_call_target="tpu_custom_call" | custom-call | tf_op jit(solution)/shard_map/pallas_call | solution.py:442
  62.6 0.8 %copy.6 = bf16[128,2048]{1,0:T(8,128)(2,1)} copy(bf16[128,2048]{1,0:T(8,128)(2,1)S(1)} %shard_map.46) | data formatting | bytes 1048576
Async XLA Ops:
  0.0 0.7 %copy-start = (f32[2048]{0:T(1024)S(1)}, f32[2048]{0:T(1024)}, u32[]{:S(2)}) copy-start(f32[2048]{0:T(1024)} %param.5) | copy-start | bytes 24580
